TPU v7x, 256 devices: a whole 4x4x8 slice. The times are simulated.
256 devices in a mesh: sp: 32 (over z, y), tp: 8 (over x, core).
Axes of the slice: x: 4, y: 4, z: 8, core: 2. Of those that a mesh axis runs over, the one named last changes fastest.
Arguments:
- block_input: bfloat16 [32768, 2048], P('sp'), may hold values from -6 to 6
- value_proj: bfloat16 [2048, 1024], P(None, 'tp'), may hold values from -0.125 to 0.125
- gate_proj: bfloat16 [2048, 1024], P(None, 'tp'), may hold values from -0.125 to 0.125
- conv_taps: float32 [31, 1024], P(None, 'tp'), may hold values from -3 to 3
- norm_gain: float32 [1024], P('tp'), may hold values from 0.1 to 1.9
- out_proj: bfloat16 [2048, 1024], P(None, 'tp'), may hold values from -0.125 to 0.125
- grad_output: bfloat16 [32768, 2048], P('sp'), may hold values from -6 to 6
Outputs:
- input_grad: bfloat16 [32768, 2048], P('sp', 'tp')
- value_grad: float32 [2048, 1024], P('sp', 'tp')
- gate_grad: float32 [2048, 1024], P('sp', 'tp')
- out_grad: float32 [2048, 1024], P('sp', 'tp')
- taps_grad: float32 [31, 1024], P(None, 'tp')
- gain_grad: float32 [1024], P('tp')
All inputs are finite; a program needn't handle non-finite values.
Results may differ from a plain program's by a relative error of at most 0.015.
Values may be sent and summed in bfloat16 or wider, within the bound.
A program may use at most 64 MiB of HBM per device.

v0:
```python
import jax
import jax.numpy as jnp
from jax import lax
from jax.sharding import Mesh
from jax.sharding import PartitionSpec as P

C = 1024
SP = ("sp_0", "sp_1")


norm_floor = 0.1


def sent_to_all(value, axis):
    count = lax.axis_size(axis)
    return lax.all_to_all(
        jnp.broadcast_to(value[None], (count, *value.shape)), axis, 0, 0, tiled=True
    )


def taken_together(value, axis):
    return sent_to_all(value, axis).sum(axis=0)


def together(arrays, axis):
    ends = [0]
    for a in arrays:
        ends.append(ends[-1] + a.size)
    so_far = taken_together(jnp.concatenate([a.ravel() for a in arrays]), axis)
    return tuple((so_far[b:e].reshape(a.shape) for a, b, e in zip(arrays, ends, ends[1:])))


def from_behind(value, axis, by):
    count = lax.axis_size(axis)
    pairs = [(i, i + by) for i in range(count) if 0 <= i + by < count]
    return lax.ppermute(value, axis, pairs)


def sum_by_axis(terms, axes):
    so_far = terms.astype(jnp.bfloat16)
    for axis in axes:
        so_far = lax.psum_scatter(so_far, axis, scatter_dimension=0, tiled=True)
    return so_far.astype(jnp.float32)


def cut_along(value, dim, count):
    dims = value.shape
    blocks = value.reshape(*dims[:dim], count, dims[dim] // count, *dims[dim + 1 :])
    return jnp.moveaxis(blocks, dim, 0)


def sent_and_summed(value, axis, dim):
    blocks = cut_along(value, dim, lax.axis_size(axis))
    arrived = lax.all_to_all(blocks, axis, split_axis=0, concat_axis=0, tiled=True)
    return arrived.astype(jnp.float32).sum(axis=0)


def causal_conv(history, conv_taps, out_rows):
    tap_count = conv_taps.shape[0]
    running = jnp.zeros((out_rows, history.shape[1]), jnp.float32)
    for tap_index in range(tap_count):
        offset = tap_count - 1 - tap_index
        running = running + conv_taps[tap_index] * history[offset : offset + out_rows].astype(
            jnp.float32
        )
    return running


def adjoint_conv(future, conv_taps, out_rows):
    tap_count = conv_taps.shape[0]
    running = jnp.zeros((out_rows, future.shape[1]), jnp.float32)
    for tap_index in range(tap_count):
        running = running + conv_taps[tap_index] * future[tap_index : tap_index + out_rows]
    return running


def tap_terms(history, conv_slope, conv_taps):
    tap_count = conv_taps.shape[0]
    out_rows = conv_slope.shape[0]
    terms = []
    for tap_index in range(tap_count):
        offset = tap_count - 1 - tap_index
        terms.append(
            jnp.sum(conv_slope * history[offset : offset + out_rows].astype(jnp.float32), axis=0)
        )
    return jnp.stack(terms)


def glu_rows(rows_in, value_proj, gate_proj):
    value_part = jnp.dot(rows_in, value_proj, preferred_element_type=jnp.float32)
    gate_part = jnp.dot(rows_in, gate_proj, preferred_element_type=jnp.float32)
    return (value_part, jax.nn.sigmoid(gate_part))


def norm_chain(history, slope, conv_taps, norm_gain, out_rows):
    conv_out = causal_conv(history, conv_taps, out_rows)
    sum_values, squares = together(
        (jnp.sum(conv_out, axis=1), jnp.sum(conv_out * conv_out, axis=1)), "tp"
    )
    center = sum_values / C
    inverse = lax.rsqrt(squares / C - center * center + norm_floor)
    normed = (conv_out - center[:, None]) * inverse[:, None]
    scaled = normed * norm_gain
    squash = jax.nn.sigmoid(scaled)
    activated = (scaled * squash).astype(jnp.bfloat16)
    pre_slope = slope * squash * (1.0 + scaled * (1.0 - squash))
    norm_slope = pre_slope * norm_gain
    slope_sum, cross_sum = together(
        (jnp.sum(norm_slope, axis=1), jnp.sum(norm_slope * normed, axis=1)), "tp"
    )
    conv_slope = inverse[:, None] * (
        norm_slope - slope_sum[:, None] / C - normed * (cross_sum[:, None] / C)
    )
    return (activated, normed, pre_slope, conv_slope)


def column_term(left_rows, right_rows):
    return lax.dot_general(
        left_rows, right_rows, (((0,), (0,)), ((), ())), preferred_element_type=jnp.float32
    )


def shards(block_input, value_proj, gate_proj, conv_taps, norm_gain, out_proj, grad_output):
    own_rows = block_input.shape[0]
    local_width = value_proj.shape[1]
    reach_rows = conv_taps.shape[0] - 1
    value_own, sgate_own = glu_rows(block_input, value_proj, gate_proj)
    mixed_own = (value_own * sgate_own).astype(jnp.bfloat16)
    slope_own = jnp.dot(grad_output, out_proj, preferred_element_type=jnp.float32)
    prior_rows = from_behind(mixed_own[own_rows - reach_rows :], SP, 1)
    history = jnp.concatenate([prior_rows, mixed_own], axis=0)
    activated, normed, pre_slope, conv_slope = norm_chain(
        history, slope_own, conv_taps, norm_gain, own_rows
    )
    blank_rows = jnp.zeros((reach_rows, local_width), jnp.float32)
    future = jnp.concatenate([blank_rows, conv_slope, blank_rows], axis=0)
    spread_slope = adjoint_conv(future, conv_taps, own_rows + reach_rows)
    returned = from_behind(spread_slope[:reach_rows], SP, -1)
    mixed_slope = spread_slope[reach_rows:].at[own_rows - reach_rows :].add(returned)
    taps_grad = tap_terms(history, conv_slope, conv_taps)
    gain_grad = jnp.sum(pre_slope * normed, axis=0)
    value_slope = (mixed_slope * sgate_own).astype(jnp.bfloat16)
    gate_slope = (mixed_slope * value_own * sgate_own * (1.0 - sgate_own)).astype(jnp.bfloat16)
    stacked = sum_by_axis(
        jnp.concatenate(
            [
                column_term(block_input, value_slope),
                column_term(block_input, gate_slope),
                column_term(grad_output, activated),
            ],
            axis=1,
        ),
        SP,
    )
    value_grad = stacked[:, :local_width]
    gate_grad = stacked[:, local_width : 2 * local_width]
    out_grad = stacked[:, 2 * local_width :]
    contract = (((1,), (1,)), ((), ()))
    partial_value = lax.dot_general(
        value_slope, value_proj, contract, preferred_element_type=jnp.float32
    )
    partial_value = partial_value + lax.dot_general(
        gate_slope, gate_proj, contract, preferred_element_type=jnp.float32
    )
    input_grad = sent_and_summed(partial_value.astype(jnp.bfloat16), "tp", 1).astype(jnp.bfloat16)
    taps_grad, gain_grad = together((taps_grad, gain_grad), SP)
    return (input_grad, value_grad, gate_grad, out_grad, taps_grad, gain_grad)


def solution(mesh):
    finer = Mesh(mesh.devices.reshape(8, 4, mesh.shape["tp"]), ("sp_0", "sp_1", "tp"))
    placed = (
        P(SP, None),
        P(None, "tp"),
        P(None, "tp"),
        P(None, "tp"),
        P("tp"),
        P(None, "tp"),
        P(SP, None),
    )
    return jax.shard_map(
        shards,
        mesh=finer,
        in_specs=placed,
        out_specs=(P(SP, "tp"), P(SP, "tp"), P(SP, "tp"), P(SP, "tp"), P(None, "tp"), P("tp")),
        check_vma=False,
    )
```

profile of v0, /device:TPU:2, one launch (start us, length us, event | category | flops | bytes accessed | tf_op | source)
XLA Modules:
  0.0 156.0 jit_solution(16820505278787248004)
XLA Ops:
  7.2 0.0 copy-start
  7.2 0.0 copy-start.1
  7.2 3.7 %fusion.6 = f32[1024,128]{1,0:T(8,128)S(1)} fusion(bf16[1024,2048]{1,0:T(8,128)(2,1)} %param.9, bf16[2048,128]{1,0:T(8,128)(2,1)} %param.11), kind=kOutput, calls=%fused_computation.43 | convolution fusion | flops 537264128 | bytes 5242880 | tf_op jit(solution)/shard_map/dot_general | solution.py:91
  10.9 0.0 copy-done
  10.9 0.0 copy-done.1
  11.0 0.0 copy-start.15
  11.0 1.3 multiply_convert_fusion.3
  12.2 3.5 %collective-permute-start = (bf16[30,128]{1,0:T(8,128)(2,1)S(1)}, bf16[30,128]{1,0:T(8,128)(2,1)S(1)}, u32[]{:S(2)}, u32[]{:S(2)}) collective-permute-start(bf16[30,128]{1,0:T(8,128)(2,1)S(1)} %slice.505), channel_id=1, source_target_pairs={{0,8},{8,16},{16,24},{24,32},{32,40},{40,48},{48,56},{56,64},{64,7... | collective-permute-start | bytes 23048 | tf_op jit(solution)/shard_map/ppermute | solution.py:36
  15.7 0.0 copy-done.5
  15.8 0.0 copy-start.6
  15.8 0.0 copy-start.7
  15.9 1.2 collective-permute-done
  17.1 2.7 %fusion.135 = (f32[1024]{0:T(1024)S(1)}, f32[1024]{0:T(1024)S(1)}, f32[1024,128]{1,0:T(8,128)S(1)}) fusion(bf16[1024,128]{1,0:T(8,128)(2,1)S(1)} %get-tuple-element.120, bf16[30,128]{1,0:T(8,128)(2,1)S(1)} %collective-permute-done, f32[128]{0:T(128)S(1)} %get-tuple-element.114, f32[128]{0:T(128)S(1)} %get-tuple-element.115, f32[128]{0:T(128)S(1)} %get-tuple-element.86, ...), kind=kLoop, calls=%fused_computation.315 | loop fusion | flops 24246272 | bytes 818176 | tf_op jit(solution)/shard_map/reduce_sum | solution.py:98
  19.9 8.8 %all_to_all.23 = f32[8,1,2048]{2,1,0:T(1,128)S(1)} all-to-all(f32[8,1,2048]{2,1,0:T(1,128)S(1)} %broadcast_in_dim.8), channel_id=1, replica_groups=mesh['sp_0'=8,'sp_1'=4,'tp'=8] {'tp'}, dimensions={0} | all-to-all | bytes 131072 | tf_op jit(solution)/shard_map/all_to_all | solution.py:16
  28.7 0.1 reduce_sum.365
  28.8 4.2 %multiply_reduce_fusion = (f32[128]{0:T(128)}, f32[1024]{0:T(1024)S(1)}, f32[1024]{0:T(1024)S(1)}, f32[1024,128]{1,0:T(8,128)S(1)}) fusion(f32[1024,128]{1,0:T(8,128)S(1)} %get-tuple-element.79, f32[1024]{0:T(1024)S(1)} %get-tuple-element.119, f32[1024]{0:T(1024)S(1)} %get-tuple-element.118, f32[128]{0:T(128)S(1)} %copy-done.15, ...), kind=kOutput, calls=%fused_computation.226 | convolution fusion | flops 539096960 | bytes 5784576 | tf_op jit(solution)/shard_map/dot_general | solution.py:129
  33.0 0.7 broadcast_in_dim.9
  33.7 4.7 %all-to-all-start.1 = ((f32[8,1,2048]{2,1,0:T(1,128)}), f32[8,1,2048]{2,1,0:T(1,128)S(1)}, u32[]{:S(2)}, u32[]{:S(2)}) async-start(f32[8,1,2048]{2,1,0:T(1,128)} %broadcast_in_dim.9), calls=%async_computation.1 | async-start | bytes 131072 | tf_op jit(solution)/shard_map/all_to_all | solution.py:16
  38.4 4.0 %fusion.2 = bf16[2048,128]{0,1:T(8,128)(2,1)} fusion(bf16[1024,2048]{1,0:T(8,128)(2,1)} %param.15, f32[1024,128]{1,0:T(8,128)S(1)} %get-tuple-element.79, f32[128]{0:T(128)S(1)} %copy-done.15, f32[1024]{0:T(1024)S(1)} %get-tuple-element.119, f32[1024]{0:T(1024)S(1)} %get-tuple-element.118), kind=kOutput, calls=%fused_computation.36 | convolution fusion | flops 538181632 | bytes 5251584 | tf_op jit(solution)/shard_map/dot_general | solution.py:118
  42.4 0.2 all-to-all-done.1
  42.6 0.1 reduce_sum.368
  42.7 1.6 %fusion.86 = (f32[128]{0:T(128)}, f32[128]{0:T(128)}, f32[128]{0:T(128)}, f32[128]{0:T(128)}, f32[128]{0:T(128)}, /*index=5*/f32[128]{0:T(128)}, f32[1024,128]{1,0:T(8,128)S(1)}) fusion(bf16[30,128]{1,0:T(8,128)(2,1)S(1)} %collective-permute-done, bf16[1024,128]{1,0:T(8,128)(2,1)S(1)} %get-tuple-element.120, f32[1024]{0:T(1024)S(1)} %get-tuple-element.117, ...), kind=kLoop, calls=%fused_computation.214 | loop fusion | flops 5635328 | bytes 1862656 | tf_op jit(solution)/shard_map/reduce_sum | solution.py:84
  44.3 0.8 concatenate.31
  45.1 2.9 %fusion.8 = f32[1054,128]{1,0:T(8,128)S(1)} fusion(f32[1084,128]{1,0:T(8,128)S(1)} %concatenate.31, f32[1024,128]{1,0:T(8,128)S(1)} %get-tuple-element.78, f32[128]{0:T(128)} %copy-done.13, f32[128]{0:T(128)} %copy-done.14, f32[128]{0:T(128)S(1)} %get-tuple-element.86, f32[128]{0:T(128)S(1)} %get-tuple-element.87, f32[128]{0:T(128)S(1)} %get-tuple-element.88, ...), kind=kLoop, calls=%fused_computation.108 | loop fusion | flops 8229632 | bytes 16729600 | tf_op jit(solution)/shard_map/add | solution.py:73
  48.0 1.3 collective-permute-start.1
  49.3 0.4 fusion.68
  49.8 0.4 fusion.74
  50.2 0.4 fusion.80
  50.7 0.5 fusion.97
  51.1 1.4 stack.127
  52.6 0.7 pad_maximum_fusion.2
  53.3 1.3 broadcast_in_dim.11
  54.5 15.0 %all-to-all-start.3 = ((f32[32,1,4096]{2,1,0:T(1,128)}), f32[32,1,4096]{2,1,0:T(1,128)S(1)}, u32[]{:S(2)}, u32[]{:S(2)}) async-start(f32[32,1,4096]{2,1,0:T(1,128)} %broadcast_in_dim.11), calls=%async_computation.4 | async-start | bytes 1048576 | tf_op jit(solution)/shard_map/all_to_all | solution.py:16
  69.5 0.2 reduce-scatter.5.cloned.1.call-start
  69.7 0.0 collective-permute-done.1
  69.8 0.2 scatter-add.4
  70.0 0.0 copy-start.2
  70.0 0.1 multiply_convert_fusion.2
  70.1 0.0 copy-start.4
  70.1 3.1 %fusion = bf16[2048,128]{0,1:T(8,128)(2,1)S(1)} fusion(bf16[1024,128]{1,0:T(8,128)(2,1)S(1)} %get-tuple-element.80, bf16[1024,2048]{1,0:T(8,128)(2,1)} %param.9), kind=kOutput, calls=%fused_computation.34 | convolution fusion | flops 537133056 | bytes 4980736 | tf_op jit(solution)/shard_map/dot_general | solution.py:118
  73.2 0.2 copy-done.2
  73.4 0.7 fusion.1
  74.2 0.0 copy-done.4
  74.2 1.3 pad_maximum_fusion
  75.5 0.0 reduce-scatter.5.cloned.1.call-update
  75.5 0.0 copy-done.3
  75.5 1.3 fusion.138
  76.8 1.3 add_convert_fusion
  78.1 2.2 %copy.44 = bf16[128,8,8,256]{3,2,0,1:T(8,128)(2,1)} copy(bf16[128,8,8,256]{3,2,1,0:T(8,128)(2,1)S(1)} %bitcast.125) | data formatting | bytes 8388608 | tf_op jit(solution)/shard_map/reshape | solution.py:48
  80.3 6.8 %all-to-all-done.3 = f32[32,1,4096]{2,1,0:T(1,128)S(1)} async-done(((f32[32,1,4096]{2,1,0:T(1,128)}), f32[32,1,4096]{2,1,0:T(1,128)S(1)}, u32[]{:S(2)}, u32[]{:S(2)}) %all-to-all-start.3) | async-done | bytes 524320 | tf_op jit(solution)/shard_map/all_to_all | solution.py:16
  87.1 5.7 %all-to-all-start.2 = ((bf16[8,1024,256]{2,1,0:T(8,128)(2,1)}), bf16[8,1024,256]{2,1,0:T(8,128)(2,1)}, u32[]{:S(2)}, u32[]{:S(2)}) async-start(bf16[8,1024,256]{2,1,0:T(8,128)(2,1)} %bitcast.126), calls=%async_computation.2 | async-start | bytes 8388608 | tf_op jit(solution)/shard_map/all_to_all | solution.py:54
  92.7 24.6 %reduce-scatter.5.cloned.1.call-done = bf16[256,384]{0,1:T(8,128)(2,1)} async-done(((bf16[2048,384]{0,1:T(8,128)(2,1)}), bf16[256,384]{0,1:T(8,128)(2,1)}) %reduce-scatter.5.cloned.1.call-update) | async-done | bytes 196624 | tf_op jit(solution)/shard_map/reduce_scatter | solution.py:42
  117.3 1.7 %copy.31 = bf16[256,384]{1,0:T(8,128)(2,1)} copy(bf16[256,384]{0,1:T(8,128)(2,1)} %reduce-scatter.5.cloned.1.call-done) | data formatting | bytes 393216
  119.1 0.0 reduce-scatter.7.cloned.1.call-update
  119.1 0.4 reduce_sum.402
  119.5 0.5 slice.604
  120.0 0.6 slice_bitcast_fusion
  120.6 21.8 %reduce-scatter.7.cloned.1.call-done = bf16[64,384]{1,0:T(8,128)(2,1)} async-done(((bf16[256,384]{1,0:T(8,128)(2,1)}), bf16[64,384]{1,0:T(8,128)(2,1)}) %reduce-scatter.7.cloned.1.call-update) | async-done | bytes 49168
  142.4 0.9 copy.32
  143.4 0.7 copy.30
  144.1 0.7 copy.29
  144.7 0.7 copy.28
  145.4 0.0 all-to-all-done.2
  145.4 3.7 %reduce_sum.369 = bf16[1024,256]{1,0:T(8,128)(2,1)} reduce(bf16[8,1024,256]{2,1,0:T(8,128)(2,1)} %all-to-all-done.2, bf16[]{:T(256)} %constant.44.clone.1), dimensions={0}, to_apply=%region_6.0 | reduce | flops 1835008 | bytes 4718594 | tf_op jit(solution)/shard_map/reduce_sum | solution.py:55
  (33 shorter events, 0.2 us)
Async XLA Ops:
  7.2 3.8 %copy-start = (bf16[2048,128]{1,0:T(8,128)(2,1)S(1)}, bf16[2048,128]{1,0:T(8,128)(2,1)}, u32[]{:S(2)}) copy-start(bf16[2048,128]{1,0:T(8,128)(2,1)} %param.10) | copy-start | bytes 1572868
  7.2 3.8 %copy-start.1 = (bf16[1024,2048]{1,0:T(8,128)(2,1)S(1)}, bf16[1024,2048]{1,0:T(8,128)(2,1)}, u32[]{:S(2)}) copy-start(bf16[1024,2048]{1,0:T(8,128)(2,1)} %param.9) | copy-start | bytes 12582916
  10.9 4.8 %copy-start.5 = (f32[31,128]{1,0:T(8,128)S(1)}, f32[31,128]{1,0:T(8,128)}, u32[]{:S(2)}) copy-start(f32[31,128]{1,0:T(8,128)} %param.12) | copy-start | bytes 47620
  11.0 17.9 %copy-start.15 = (f32[128]{0:T(128)S(1)}, f32[128]{0:T(128)}, u32[]{:S(2)}) copy-start(f32[128]{0:T(128)} %param.13) | copy-start | bytes 1540
  12.2 4.8 %collective-permute-start = (bf16[30,128]{1,0:T(8,128)(2,1)S(1)}, bf16[30,128]{1,0:T(8,128)(2,1)S(1)}, u32[]{:S(2)}, u32[]{:S(2)}) collective-permute-start(bf16[30,128]{1,0:T(8,128)(2,1)S(1)} %slice.505), channel_id=1, source_target_pairs={{0,8},{8,16},{16,24},{24,32},{32,40},{40,48},{48,56},{56,64},{64,7... | collective-permute-start | bytes 23048 | tf_op jit(solution)/shard_map/ppermute | solution.py:36
  15.8 4.0 %copy-start.6 = (f32[128]{0:T(128)}, f32[128]{0:T(128)S(1)}, u32[]{:S(2)}) copy-start(f32[128]{0:T(128)S(1)} %get-tuple-element.107) | copy-start | bytes 1540
  15.8 4.0 %copy-start.7 = (f32[128]{0:T(128)}, f32[128]{0:T(128)S(1)}, u32[]{:S(2)}) copy-start(f32[128]{0:T(128)S(1)} %get-tuple-element.108) | copy-start | bytes 1540
  15.8 4.0 %copy-start.8 = (f32[128]{0:T(128)}, f32[128]{0:T(128)S(1)}, u32[]{:S(2)}) copy-start(f32[128]{0:T(128)S(1)} %get-tuple-element.109) | copy-start | bytes 1540
  15.8 4.0 %copy-start.9 = (f32[128]{0:T(128)}, f32[128]{0:T(128)S(1)}, u32[]{:S(2)}) copy-start(f32[128]{0:T(128)S(1)} %get-tuple-element.110) | copy-start | bytes 1540
  15.8 4.0 %copy-start.10 = (f32[128]{0:T(128)}, f32[128]{0:T(128)S(1)}, u32[]{:S(2)}) copy-start(f32[128]{0:T(128)S(1)} %get-tuple-element.111) | copy-start | bytes 1540
  15.8 4.0 %copy-start.11 = (f32[128]{0:T(128)}, f32[128]{0:T(128)S(1)}, u32[]{:S(2)}) copy-start(f32[128]{0:T(128)S(1)} %get-tuple-element.112) | copy-start | bytes 1540
  15.8 4.0 %copy-start.12 = (f32[128]{0:T(128)}, f32[128]{0:T(128)S(1)}, u32[]{:S(2)}) copy-start(f32[128]{0:T(128)S(1)} %get-tuple-element.113) | copy-start | bytes 1540
  15.8 4.0 %copy-start.13 = (f32[128]{0:T(128)}, f32[128]{0:T(128)S(1)}, u32[]{:S(2)}) copy-start(f32[128]{0:T(128)S(1)} %get-tuple-element.114) | copy-start | bytes 1540
  15.9 4.0 %copy-start.14 = (f32[128]{0:T(128)}, f32[128]{0:T(128)S(1)}, u32[]{:S(2)}) copy-start(f32[128]{0:T(128)S(1)} %get-tuple-element.115) | copy-start | bytes 1540
  33.7 8.9 %all-to-all-start.1 = ((f32[8,1,2048]{2,1,0:T(1,128)}), f32[8,1,2048]{2,1,0:T(1,128)S(1)}, u32[]{:S(2)}, u32[]{:S(2)}) async-start(f32[8,1,2048]{2,1,0:T(1,128)} %broadcast_in_dim.9), calls=%async_computation.1 | async-start | bytes 131072 | tf_op jit(solution)/shard_map/all_to_all | solution.py:16
  48.0 21.7 %collective-permute-start.1 = (f32[30,128]{1,0:T(8,128)S(1)}, f32[30,128]{1,0:T(8,128)S(1)}, u32[]{:S(2)}, u32[]{:S(2)}) collective-permute-start(f32[30,128]{1,0:T(8,128)S(1)} %slice.599), channel_id=1, source_target_pairs={{8,0},{16,8},{24,16},{32,24},{40,32},{48,40},{56,48},{64,56},{72,6... | collective-permute-start | bytes 46088 | tf_op jit(solution)/shard_map/ppermute | solution.py:36
  54.5 32.5 %all-to-all-start.3 = ((f32[32,1,4096]{2,1,0:T(1,128)}), f32[32,1,4096]{2,1,0:T(1,128)S(1)}, u32[]{:S(2)}, u32[]{:S(2)}) async-start(f32[32,1,4096]{2,1,0:T(1,128)} %broadcast_in_dim.11), calls=%async_computation.4 | async-start | bytes 1048576 | tf_op jit(solution)/shard_map/all_to_all | solution.py:16
  69.5 47.8 %reduce-scatter.5.cloned.1.call-start = ((), (), s32[]{:S(2)}) async-start(), calls=%async_computation.6 | async-start | bytes 1769472 | tf_op jit(solution)/shard_map/reduce_scatter | solution.py:42
  70.0 3.5 %copy-start.2 = (bf16[1024,2048]{1,0:T(8,128)(2,1)S(1)}, bf16[1024,2048]{1,0:T(8,128)(2,1)}, u32[]{:S(2)}) copy-start(bf16[1024,2048]{1,0:T(8,128)(2,1)} %param.9) | copy-start | bytes 12582916
  70.1 4.1 %copy-start.4 = (bf16[2048,128]{0,1:T(8,128)(2,1)S(1)}, bf16[2048,128]{0,1:T(8,128)(2,1)}, u32[]{:S(2)}) copy-start(bf16[2048,128]{0,1:T(8,128)(2,1)} %fusion.2) | copy-start | bytes 1572868
  73.4 2.1 %copy-start.3 = (bf16[2048,128]{1,0:T(8,128)(2,1)S(1)}, bf16[2048,128]{1,0:T(8,128)(2,1)}, u32[]{:S(2)}) copy-start(bf16[2048,128]{1,0:T(8,128)(2,1)} %param.11) | copy-start | bytes 1572868
  87.1 58.4 %all-to-all-start.2 = ((bf16[8,1024,256]{2,1,0:T(8,128)(2,1)}), bf16[8,1024,256]{2,1,0:T(8,128)(2,1)}, u32[]{:S(2)}, u32[]{:S(2)}) async-start(bf16[8,1024,256]{2,1,0:T(8,128)(2,1)} %bitcast.126), calls=%async_computation.2 | async-start | bytes 8388608 | tf_op jit(solution)/shard_map/all_to_all | solution.py:54
  92.7 49.7 %reduce-scatter.7.cloned.1.call-start = ((), (), s32[]{:S(2)}) async-start(), calls=%async_computation.7 | async-start | bytes 245760
Sparse Core Ops, SparseCore 0:
  75.6 41.6 reduce-scatter.4
  120.4 21.9 reduce-scatter.6
where the time goes:
time: 157 us; the launch traced here: 156 us
  waiting for transfers between devices  54.6 us (35%)
  starting transfers between devices  30.4 us (19%)
  matrix products  19.5 us (12%)
  other arithmetic  15.3 us (10%)
  between operations  14.5 us (9%)
  local copies, waits for them, and re-layouts  12.9 us (8%)
  blocking collectives  8.79 us (6%)
    reduce_scatter x1, waiting for transfers between devices, sum_by_axis(): so_far = lax.psum_scatter(so_far, axis, scatter_dimension=0, tiled=True)  24.6 us
    unnamed x3, waiting for transfers between devices  21.8 us
    all_to_all x2, starting transfers between devices, sent_to_all(): lax.all_to_all(jnp.broadcast_to(value[None], (count, *value.shape)), axis...  19.7 us
    all_to_all x1, blocking collectives, sent_to_all(): lax.all_to_all(jnp.broadcast_to(value[None], (count, *value.shape)), axis...  8.79 us
    dot_general x3, matrix products, column_term(): lax.dot_general(left_rows, right_rows, (((0,), (0,)), ((), ())), preferre...  7.83 us
    all_to_all x2, waiting for transfers between devices, sent_to_all(): lax.all_to_all(jnp.broadcast_to(value[None], (count, *value.shape)), axis...  6.96 us
    all_to_all x1, starting transfers between devices, sent_and_summed(): lax.all_to_all(blocks, axis, split_axis=0, concat_axis=0, tiled=True)  5.69 us
    unnamed x37, local copies, waits for them, and re-layouts  5.05 us
  transfers between devices with their start and end apart: 7, of which 5 were waited for; matrix products, arithmetic and copies ran while one was open for 16% of the time, Pallas kernels for 0%

commit v1 on v0

v1 whole, which is shorter than its diff:
```python
import functools

import jax
import jax.numpy as jnp
from jax import lax
from jax.experimental import pallas as pl
from jax.experimental.pallas import tpu as pltpu
from jax.sharding import Mesh
from jax.sharding import PartitionSpec as P

MESH = pl.DeviceIdType.MESH
F32 = jnp.float32
BF16 = jnp.bfloat16
norm_floor = 0.1
L = 128
S = 8
J = 8
PAD = 32
NC = 4


def dot_nn(a, b):
    return lax.dot_general(a, b, (((1,), (0,)), ((), ())), preferred_element_type=F32)


def dot_nt(a, b):
    return lax.dot_general(a, b, (((1,), (1,)), ((), ())), preferred_element_type=F32)


def body(
    Z, Y, C, K,
    x_hbm, vp_hbm, gp_hbm, taps, gain, op_hbm, g_hbm,
    ig, vg, gg, og, tg, ng,
    xv, gv, wvg, wo, wg, vbuf, sbuf, slope, hist, convp, nrm, nsl, act, cs, vsf, gsf, sl, slg, acc,
    actT, slT, wgo, wgv, yro, yrv, zso, zsv, zro, zrv, sta, star, stb, stbr, tgs, tgy, tgzs, tgz,
    l_sem, x_sem, g_sem, w_ss, w_rs, h_ss, h_rs, sa_ss, sa_rs, sb_ss, sb_rs, own_ss, fwd_ss, pf_ss, slg_rs,
    yo_ss, yo_rs, yv_ss, yv_rs, zo_ss, zo_rs, zv_ss, zv_rs, ty_ss, ty_rs, tz_ss, tz_rs, ow_sem,
):
    z, y, x, c = (lax.axis_index(a) for a in ("z", "y", "x", "c"))
    rows, D = xv.shape
    T = rows // S
    DB = D // 8
    RB = D // (Z * Y)
    CH = rows // NC
    H = K - 1

    yn = (y + 1) % Y
    zn = (z + (y + 1) // Y) % Z
    yb = (y + Y - 1) % Y
    zb = (z + Z - 1 + (y + Y - 1) // Y) % Z
    first = (z + y) == 0
    last = (z * Y + y) == (Z * Y - 1)
    xp, xm = (x + 1) % 4, (x + 3) % 4
    xs = (x, x + 1 - 2 * (x % 2), (x + 2) % 4, 3 - x)
    cc = (c, 1 - c)

    def to(z=z, y=y, x=x, c=c):
        return {"z": z, "y": y, "x": x, "c": c}

    def remote(src, dst, ss, rs, dev):
        return pltpu.make_async_remote_copy(
            src_ref=src, dst_ref=dst, send_sem=ss, recv_sem=rs, device_id=dev, device_id_type=MESH
        )

    tp_peers = [to(x=xs[o // 2], c=cc[o % 2]) for o in range(1, 8)]
    y_peers = [to(y=(y + d) % Y) for d in range(1, Y)]
    z_peers = [to(z=(z + d) % Z) for d in range(1, Z)]
    nxt, prv = to(z=zn, y=yn), to(z=zb, y=yb)
    sent = []

    loads = [
        pltpu.make_async_copy(vp_hbm, wvg.at[:, pl.ds(0, L)], l_sem.at[0]),
        pltpu.make_async_copy(gp_hbm, wvg.at[:, pl.ds(L, L)], l_sem.at[1]),
        pltpu.make_async_copy(op_hbm, wo, l_sem.at[2]),
    ]
    loads[0].start()
    loads[1].start()
    XC = 4
    XR = rows // XC

    def x_load(i):
        at = pl.ds(pl.multiple_of(i * XR, XR), XR)
        return pltpu.make_async_copy(x_hbm.at[at], xv.at[at], x_sem.at[i])

    def g_load(i):
        at = pl.ds(pl.multiple_of(i * XR, XR), XR)
        return pltpu.make_async_copy(g_hbm.at[at], gv.at[at], g_sem.at[i])

    for i in (XC - 1, *range(XC - 1)):
        x_load(i).start()
    loads[2].start()
    for i in range(XC):
        g_load(i).start()

    barrier = pltpu.get_barrier_semaphore()
    greet = [*tp_peers, *y_peers, *z_peers, nxt, prv]
    for dev in greet:
        pl.semaphore_signal(barrier, inc=1, device_id=dev, device_id_type=MESH)
    pl.semaphore_wait(barrier, len(greet))

    loads[0].wait()
    loads[1].wait()

    w_copies = []
    for o in range(1, 8):
        px, pc = xs[o // 2], cc[o % 2]
        at = pl.ds(pl.multiple_of((px * 2 + pc) * DB, DB), DB)
        w_copies.append(remote(wvg.at[at], wg.at[o - 1], w_ss.at[o - 1], w_rs.at[o - 1], tp_peers[o - 1]))
    for cp in w_copies:
        cp.start()

    def x_step(i):
        x_load(i).wait()
        at = pl.ds(pl.multiple_of(i * XR, XR), XR)
        res = dot_nn(xv[at, :], wvg[...])
        v = res[:, :L]
        s = jax.nn.sigmoid(res[:, L:])
        vbuf[at, :] = v
        sbuf[at, :] = s
        hist[pl.ds(pl.multiple_of(PAD + i * XR, PAD), XR), :] = (v * s).astype(BF16).astype(F32)

    x_step(XC - 1)
    halo_m = remote(hist.at[pl.ds(rows, PAD)], hist.at[pl.ds(0, PAD)], h_ss.at[0], h_rs.at[0], nxt)
    halo_m.start()

    def x_loop(i, carry):
        x_step(i)
        return carry

    lax.fori_loop(0, XC - 1, x_loop, 0)
    loads[2].wait()

    def g_loop(i, carry):
        g_load(i).wait()
        at = pl.ds(pl.multiple_of(i * XR, XR), XR)
        slope[at, :] = dot_nn(gv[at, :], wo[...])
        return carry

    lax.fori_loop(0, XC, g_loop, 0)

    halo_m.wait_recv()

    @pl.when(first)
    def _():
        hist[pl.ds(0, PAD), :] = jnp.zeros((PAD, L), F32)

    lane = lax.broadcasted_iota(jnp.int32, (S, L), 1)
    zero = jnp.zeros((S, L), F32)

    def rows_of(ref, t):
        return ref[pl.ds(t, S, stride=T), :]

    def spread(stat, t):
        return jnp.sum(jnp.where(lane == t, stat, 0.0), axis=1, keepdims=True)

    def tap(k):
        return taps[pl.ds(k, 1), :]

    def conv_block(b, carry):
        s1, s2 = carry
        t0 = b * J
        m = [rows_of(hist, t0 + (PAD - H) + i) for i in range(J + H)]
        for j in range(J):
            r = tap(0) * m[H + j]
            for k in range(1, K):
                r = r + tap(k) * m[H + j - k]
            convp[t0 + j] = r
            s1 = jnp.where(lane == t0 + j, jnp.sum(r, axis=1, keepdims=True), s1)
            s2 = jnp.where(lane == t0 + j, jnp.sum(r * r, axis=1, keepdims=True), s2)
        return s1, s2

    def exchange(own, got, ss, rs):
        copies = [remote(own, got.at[i], ss.at[i], rs.at[i], tp_peers[i]) for i in range(7)]
        for cp in copies:
            cp.start()
        sent.extend(copies)
        return copies

    def total(own, got, i):
        r = own[i]
        for p in range(7):
            r = r + got[p, i]
        return r * (1.0 / C)

    s1, s2 = lax.fori_loop(0, T // J, conv_block, (zero, zero))
    sta[0] = s1
    sta[1] = s2
    ex = exchange(sta, star, sa_ss, sa_rs)
    for cp in ex:
        cp.wait_recv()
    center = total(sta, star, 0)
    inverse = lax.rsqrt(total(sta, star, 1) - center * center + norm_floor)
    gains = gain[...]

    def norm_block(b, carry):
        gsum, s1, s2 = carry
        t0 = b * J
        for j in range(J):
            t = t0 + j
            n = (convp[t] - spread(center, t)) * spread(inverse, t)
            sc = n * gains
            sq = jax.nn.sigmoid(sc)
            act[pl.ds(t, S, stride=T), :] = sc * sq
            ps = rows_of(slope, t) * sq * (1.0 + sc * (1.0 - sq))
            gsum = gsum + ps * n
            ns = ps * gains
            nrm[t] = n
            nsl[t] = ns
            s1 = jnp.where(lane == t, jnp.sum(ns, axis=1, keepdims=True), s1)
            s2 = jnp.where(lane == t, jnp.sum(ns * n, axis=1, keepdims=True), s2)
        return gsum, s1, s2

    gsum, s1, s2 = lax.fori_loop(0, T // J, norm_block, (zero, zero, zero))
    stb[0] = s1
    stb[1] = s2
    ex = exchange(stb, stbr, sb_ss, sb_rs)

    def flip(src, dst, row0):
        def step(i, carry):
            at = pl.multiple_of(i * L, L)
            dst[pl.ds(row0, L), pl.ds(at, L)] = src[pl.ds(at, L), :].T.astype(BF16)
            return carry

        lax.fori_loop(0, rows // L, step, 0)

    flip(act, actT, 0)

    def weight_grad(left, right, dst):
        def step(zi, carry):
            at = pl.ds(pl.multiple_of(zi * (D // Z), D // Z), D // Z)
            r = dot_nn(left[...], right[:, at]).T.astype(BF16)
            for yi in range(Y):
                dst[zi, yi] = r[yi * RB : (yi + 1) * RB, :]
            return carry

        lax.fori_loop(0, Z, step, 0)

    def y_send(src, dst, ss, rs):
        copies = []
        for d in range(1, Y):
            copies.append(
                remote(src.at[:, (y + d) % Y], dst.at[d - 1], ss.at[d - 1], rs.at[d - 1], y_peers[d - 1])
            )
            copies[-1].start()
        sent.extend(copies)
        return copies

    weight_grad(actT, gv, wgo)
    yo = y_send(wgo, yro, yo_ss, yo_rs)

    for cp in ex:
        cp.wait_recv()
    slope_sum = total(stb, stbr, 0)
    cross_sum = total(stb, stbr, 1)

    def cs_block(b, carry):
        t0 = b * J
        for j in range(J):
            t = t0 + j
            cs[pl.ds(t, S, stride=T), :] = spread(inverse, t) * (
                nsl[t] - spread(slope_sum, t) - nrm[t] * spread(cross_sum, t)
            )
        return carry

    lax.fori_loop(0, PAD // J, cs_block, 0)
    halo_c = remote(cs.at[pl.ds(0, PAD)], cs.at[pl.ds(rows, PAD)], h_ss.at[1], h_rs.at[1], prv)
    halo_c.start()
    lax.fori_loop(PAD // J, T // J, cs_block, 0)

    def tap_block(b, sums):
        sums = list(sums)
        t0 = b * J
        m = [rows_of(hist, t0 + (PAD - H) + i) for i in range(J + H)]
        for j in range(J):
            e = rows_of(cs, t0 + j)
            for k in range(K):
                sums[k] = sums[k] + e * m[H + j - k]
        return tuple(sums)

    sums = lax.fori_loop(0, T // J, tap_block, tuple(zero for _ in range(K)))
    for k in range(K):
        tgs[pl.ds(k, 1), :] = jnp.sum(sums[k], axis=0, keepdims=True)
    tgs[pl.ds(K, 1), :] = jnp.sum(gsum, axis=0, keepdims=True)
    ty = []
    for d in range(1, Y):
        ty.append(remote(tgs, tgy.at[y], ty_ss.at[d - 1], ty_rs.at[d - 1], y_peers[d - 1]))
        ty[-1].start()
    sent.extend(ty)
    tgy[y] = tgs[...]

    halo_c.wait_recv()

    @pl.when(last)
    def _():
        cs[pl.ds(rows, PAD), :] = jnp.zeros((PAD, L), F32)

    def slope_block(b, carry):
        t0 = b * J
        f = [rows_of(cs, t0 + i) for i in range(J + H)]
        for j in range(J):
            t = t0 + j
            r = tap(0) * f[j]
            for k in range(1, K):
                r = r + tap(k) * f[j + k]
            s = rows_of(sbuf, t)
            rs = r * s
            vsf[pl.ds(t, S, stride=T), :] = rs
            gsf[pl.ds(t, S, stride=T), :] = rs * rows_of(vbuf, t) * (1.0 - s)
        return carry

    lax.fori_loop(0, T // J, slope_block, 0)
    sl[:, pl.ds(0, L)] = vsf[...].astype(BF16)
    sl[:, pl.ds(L, L)] = gsf[...].astype(BF16)

    def piece(ref, q):
        return ref.at[pl.ds(q * CH, CH)]

    def own_copy(way, slot, q, dev):
        return remote(piece(sl, q), piece(slg.at[slot], q), own_ss.at[way, q], slg_rs.at[slot, q], dev)

    right, left = to(x=xp), to(x=xm)
    partner = to(c=1 - c)
    up = [own_copy(0, 1, q, right) for q in range(NC)]
    down = [own_copy(1, 2, q, left) for q in range(NC)]
    over = [own_copy(2, 0, q, partner) for q in range(NC)]
    half = NC // 2
    for i in range(NC):
        up[i].start()
        down[(i + half) % NC].start()
    for i in range(NC):
        over[i].start()
    sent.extend([*up, *down, *over])

    flip(vsf, slT, 0)
    flip(gsf, slT, L)
    weight_grad(slT, xv, wgv)
    yv = y_send(wgv, yrv, yv_ss, yv_rs)

    for cp in w_copies:
        cp.wait_recv()
    sent.extend(w_copies)

    def weights_from(slot):
        core = 1 if slot == 0 or slot > 3 else 0
        base = slot if slot <= 3 else slot - 3
        if base == 0:
            return wg[0]
        if base == 3:
            return wg[3 + core]
        way = 3 - 2 * (x % 2) if base == 1 else 1 + 2 * (x % 2)
        return wg[2 * way + core - 1]

    at = pl.ds(pl.multiple_of((x * 2 + c) * DB, DB), DB)
    acc[...] = dot_nt(sl[...], wvg[at, :])

    def add(slot, q):
        at = pl.ds(q * CH, CH)
        acc[at, :] += dot_nt(slg[slot, at, :], weights_from(slot))

    def pf(slot, q):
        cp = remote(
            piece(slg.at[slot], q), piece(slg.at[slot + 3], q), pf_ss.at[slot - 1, q], slg_rs.at[slot + 3, q], partner
        )
        cp.start()
        sent.append(cp)
        return cp

    fwd = {}
    pfs = {}
    for i in range(NC):
        q = i
        up[q].wait_recv()
        if i < half:
            fwd[q] = remote(piece(slg.at[1], q), piece(slg.at[3], q), fwd_ss.at[q], slg_rs.at[3, q], right)
            fwd[q].start()
        pfs[1, q] = pf(1, q)
        q2 = (i + half) % NC
        down[q2].wait_recv()
        if i < half:
            fwd[q2] = remote(piece(slg.at[2], q2), piece(slg.at[3], q2), fwd_ss.at[q2], slg_rs.at[3, q2], left)
            fwd[q2].start()
        pfs[2, q2] = pf(2, q2)
        over[i].wait_recv()
        add(0, i)
        add(1, q)
        add(2, q2)
        if i == 2:
            for cp in yo:
                cp.wait_recv()
            zo = second(Z, Y, y, z, wgo, yro, zso, zro, zo_ss, zo_rs, z_peers, remote, sent)
            for cp in ty:
                cp.wait_recv()
            t = tgy[0]
            for yi in range(1, Y):
                t = t + tgy[yi]
            tgzs[...] = t
            tgz[z] = t
            tz = []
            for d in range(1, Z):
                tz.append(remote(tgzs, tgz.at[z], tz_ss.at[d - 1], tz_rs.at[d - 1], z_peers[d - 1]))
                tz[-1].start()
            sent.extend(tz)
    sent.extend(fwd.values())
    for i in range(NC):
        add_q = i
        pfs[1, add_q].wait_recv()
        add(4, add_q)
        pfs[2, add_q].wait_recv()
        add(5, add_q)

    for cp in yv:
        cp.wait_recv()
    zv = second(Z, Y, y, z, wgv, yrv, zsv, zrv, zv_ss, zv_rs, z_peers, remote, sent)

    order = [q for i in range(half) for q in (i, i + half)]
    for q in order:
        fwd[q].wait_recv()
        pfs[3, q] = pf(3, q)
        add(3, q)
    for q in order:
        pfs[3, q].wait_recv()
        add(6, q)
    ig[...] = acc[...].astype(BF16)

    for cp in zo:
        cp.wait_recv()
    r = zso[z].astype(F32)
    for d in range(1, Z):
        r = r + zro[d - 1].astype(F32)
    og[...] = r
    for cp in tz:
        cp.wait_recv()
    t = tgz[0]
    for zi in range(1, Z):
        t = t + tgz[zi]
    tg[...] = t[:K]
    ng[...] = t[K : K + 1]
    for cp in zv:
        cp.wait_recv()
    r = zsv[z].astype(F32)
    for d in range(1, Z):
        r = r + zrv[d - 1].astype(F32)
    vg[...] = r[:, :L]
    gg[...] = r[:, L:]

    for cp in [halo_m, halo_c, *sent]:
        cp.wait_send()


def second(Z, Y, y, z, own, got, zs, zr, ss, rs, z_peers, remote, sent):
    def step(zi, carry):
        r = own[zi, y].astype(F32)
        for d in range(Y - 1):
            r = r + got[d, zi].astype(F32)
        zs[zi] = r.astype(BF16)
        return carry

    lax.fori_loop(0, Z, step, 0)
    copies = []
    for d in range(1, Z):
        copies.append(remote(zs.at[(z + d) % Z], zr.at[d - 1], ss.at[d - 1], rs.at[d - 1], z_peers[d - 1]))
        copies[-1].start()
    sent.extend(copies)
    return copies


def shards(Z, Y, block_input, value_proj, gate_proj, conv_taps, norm_gain, out_proj, grad_output):
    rows, D = block_input.shape
    K = conv_taps.shape[0]
    C = value_proj.shape[1] * 8
    DB, RB, T = D // 8, D // (Z * Y), rows // S
    vm = pltpu.VMEM
    dma = pltpu.SemaphoreType.DMA
    any_, vmem = pl.BlockSpec(memory_space=pl.ANY), pl.BlockSpec(memory_space=pltpu.VMEM)
    scratch = [
        vm((rows, D), BF16), vm((rows, D), BF16), vm((D, 2 * L), BF16), vm((D, L), BF16), vm((7, DB, 2 * L), BF16),
        vm((rows, L), F32), vm((rows, L), F32), vm((rows, L), F32), vm((rows + PAD, L), F32),
        vm((T, S, L), F32), vm((T, S, L), F32), vm((T, S, L), F32), vm((rows, L), F32), vm((rows + PAD, L), F32),
        vm((rows, L), F32), vm((rows, L), F32), vm((rows, 2 * L), BF16), vm((7, rows, 2 * L), BF16), vm((rows, DB), F32),
        vm((L, rows), BF16), vm((2 * L, rows), BF16),
        vm((Z, Y, RB, L), BF16), vm((Z, Y, RB, 2 * L), BF16),
        vm((Y - 1, Z, RB, L), BF16), vm((Y - 1, Z, RB, 2 * L), BF16),
        vm((Z, RB, L), BF16), vm((Z, RB, 2 * L), BF16), vm((Z - 1, RB, L), BF16), vm((Z - 1, RB, 2 * L), BF16),
        vm((2, S, L), F32), vm((7, 2, S, L), F32), vm((2, S, L), F32), vm((7, 2, S, L), F32),
        vm((PAD, L), F32), vm((Y, PAD, L), F32), vm((PAD, L), F32), vm((Z, PAD, L), F32),
        dma((3,)), dma((4,)), dma((4,)), dma((7,)), dma((7,)), dma((2,)), dma((2,)),
        dma((7,)), dma((7,)), dma((7,)), dma((7,)), dma((3, NC)), dma((NC,)), dma((3, NC)), dma((7, NC)),
        *[dma((Y - 1,)) for _ in range(4)], *[dma((Z - 1,)) for _ in range(4)],
        dma((Y - 1,)), dma((Y - 1,)), dma((Z - 1,)), dma((Z - 1,)), dma((1,)),
    ]
    outs = pl.pallas_call(
        functools.partial(body, Z, Y, C, K),
        out_shape=(
            jax.ShapeDtypeStruct((rows, DB), BF16),
            jax.ShapeDtypeStruct((RB, L), F32),
            jax.ShapeDtypeStruct((RB, L), F32),
            jax.ShapeDtypeStruct((RB, L), F32),
            jax.ShapeDtypeStruct((K, L), F32),
            jax.ShapeDtypeStruct((1, L), F32),
        ),
        in_specs=[any_, any_, any_, vmem, vmem, any_, any_],
        out_specs=[vmem] * 6,
        scratch_shapes=scratch,
        compiler_params=pltpu.CompilerParams(
            collective_id=0, has_side_effects=True, vmem_limit_bytes=56 * 1024 * 1024
        ),
        name="block_backward",
    )(block_input, value_proj, gate_proj, conv_taps, norm_gain.reshape(1, L), out_proj, grad_output)
    return (*outs[:5], outs[5].reshape(L))


def solution(mesh):
    tp = mesh.shape["tp"]
    Y = 4
    Z = mesh.shape["sp"] // Y
    finer = Mesh(mesh.devices.reshape(Z, Y, tp // 2, 2), ("z", "y", "x", "c"))
    sp, ch = ("z", "y"), ("x", "c")
    return jax.shard_map(
        functools.partial(shards, Z, Y),
        mesh=finer,
        in_specs=(P(sp, None), P(None, ch), P(None, ch), P(None, ch), P(ch), P(None, ch), P(sp, None)),
        out_specs=(P(sp, ch), P(sp, ch), P(sp, ch), P(sp, ch), P(None, ch), P(ch)),
        check_vma=False,
    )
```

time: 157 us -> 79.4 us (0.51)
  Pallas kernels: 0 us -> 69.4 us
  waiting for transfers between devices: 54.6 us -> 0 us
  starting transfers between devices: 30.4 us -> 0 us
  matrix products: 19.5 us -> 0 us
  other arithmetic: 15.3 us -> 0 us
  between operations: 14.5 us -> 0.64 us
  blocking collectives: 8.79 us -> 0 us
  local copies, waits for them, and re-layouts: 12.9 us -> 8.43 us
    pallas_call x0 -> x1, Pallas kernels: none -> 69.4 us  [shards(): pl.pallas_call(functools.partial(body, Z, Y, C, K), out_shape=(jax.ShapeD...]
    all_to_all x3 -> x0, starting transfers between devices: 25.4 us -> none  [the longest x2 19.7 us: sent_to_all(): lax.all_to_all(jnp.broadcast_to(value[None], (count, *value.shape)), axis...]
    reduce_scatter x1 -> x0, waiting for transfers between devices: 24.6 us -> none  [sum_by_axis(): so_far = lax.psum_scatter(so_far, axis, scatter_dimension=0, tiled=True)]
    unnamed x3 -> x0, waiting for transfers between devices: 21.8 us -> none
    dot_general x8 -> x0, matrix products: 19.5 us -> none  [the longest x3 7.83 us: column_term(): lax.dot_general(left_rows, right_rows, (((0,), (0,)), ((), ())), preferre...]
    reduce_sum x10 -> x0, other arithmetic: 10.3 us -> none  [the longest x1 3.7 us: sent_and_summed(): return arrived.astype(jnp.float32).sum(axis=0)]
    all_to_all x1 -> x0, blocking collectives: 8.79 us -> none  [sent_to_all(): lax.all_to_all(jnp.broadcast_to(value[None], (count, *value.shape)), axis...]
    all_to_all x3 -> x0, waiting for transfers between devices: 6.96 us -> none  [the longest x2 6.96 us: sent_to_all(): lax.all_to_all(jnp.broadcast_to(value[None], (count, *value.shape)), axis...]
  transfers between devices with their start and end apart: 7 -> 0, of which waited for: 5 -> 0; matrix products, arithmetic and copies ran while one was open for 16% -> 0% of each run, Pallas kernels for 0% -> 0%
where the time goes in v1:
time: 79.4 us; the launch traced here: 78.5 us
  Pallas kernels  69.4 us (87%)
  local copies, waits for them, and re-layouts  8.43 us (11%)
    pallas_call x1, Pallas kernels, shards(): pl.pallas_call(functools.partial(body, Z, Y, C, K), out_shape=(jax.ShapeD...  69.4 us
    unnamed x6, local copies, waits for them, and re-layouts  8.43 us

profile of v1, /device:TPU:2, one launch (start us, length us, event | category | flops | bytes accessed | tf_op | source)
XLA Modules:
  0.0 78.5 jit_solution(17386743164352234242)
XLA Ops:
  0.6 69.4 %block_backward.1 = (bf16[1024,256]{1,0:T(8,128)(2,1)}, f32[64,128]{1,0:T(8,128)}, f32[64,128]{1,0:T(8,128)}, f32[64,128]{1,0:T(8,128)}, f32[31,128]{1,0:T(8,128)}, /*index=5*/f32[1,128]{1,0:T(1,128)}) custom-call(bf16[1024,2048]{1,0:T(8,128)(2,1)} %x_hbm.1, bf16[2048,128]{1,0:T(8,128)(2,1)} %vp_hbm.1, bf16[2048,128]{1,0:T(8,128)(2,1)} %gp_hbm.1, ...), custom_call_target="tpu_custom_call" | custom-call | tf_op jit(solution)/shard_map/block_backward/pallas_call | solution.py:491
  70.0 1.9 %copy.19 = bf16[1024,256]{1,0:T(8,128)(2,1)} copy(bf16[1024,256]{1,0:T(8,128)(2,1)} %get-tuple-element.24) | data formatting | bytes 1048576
  71.9 1.4 %copy.20 = f32[64,128]{1,0:T(8,128)} copy(f32[64,128]{1,0:T(8,128)} %get-tuple-element.25) | data formatting | bytes 65536
  73.3 1.4 %copy.21 = f32[64,128]{1,0:T(8,128)} copy(f32[64,128]{1,0:T(8,128)} %get-tuple-element.26) | data formatting | bytes 65536
  74.7 1.4 %copy.22 = f32[64,128]{1,0:T(8,128)} copy(f32[64,128]{1,0:T(8,128)} %get-tuple-element.27) | data formatting | bytes 65536
  76.0 1.3 %copy.23 = f32[31,128]{1,0:T(8,128)} copy(f32[31,128]{1,0:T(8,128)} %get-tuple-element.28) | data formatting | bytes 31744
  77.4 1.1 %copy.24 = f32[128]{0:T(128)} copy(f32[128]{0:T(128)} %bitcast.3) | data formatting | bytes 1024

commit v2 on v1

v2 whole, which is shorter than its diff:
```python
import functools

import jax
import jax.numpy as jnp
from jax import lax
from jax.experimental import pallas as pl
from jax.experimental.pallas import tpu as pltpu
from jax.sharding import Mesh
from jax.sharding import PartitionSpec as P

MESH = pl.DeviceIdType.MESH
F32 = jnp.float32
BF16 = jnp.bfloat16
norm_floor = 0.1
ANYWHERE = pltpu.HBM
VMEM_LIMIT = 40 * 1024 * 1024
L = 128
S = 8
J = 16
NP = 132
HP = 164
PAD = 32
NC = 4


def dot_nn(a, b):
    return lax.dot_general(a, b, (((1,), (0,)), ((), ())), preferred_element_type=F32)


def dot_nt(a, b):
    return lax.dot_general(a, b, (((1,), (1,)), ((), ())), preferred_element_type=F32)


def body(
    Z, Y, C, K,
    x_hbm, vp_hbm, gp_hbm, taps, gain, op_hbm, g_hbm,
    ig, vg, gg, og, tg, ng,
    xv, gv, wvg, wo, wg, vbuf, sbuf, slope, hist, convp, nrm, nsl, inv, act, cs, vsf, gsf, sl, slg, acc,
    tail, halo_in, halo_out, halo_back,
    actT, slT, wgo, wgv, wgg, yro, yrv, zso, zsv, zro, zrv, zrg, ysg, yrg, sta, star, stb, stbr, tgs, tgy, tgzs, tgz,
    l_sem, x_sem, g_sem, wo_ss, wo_rs, w_ss, w_rs, wy_ss, wy_rs, h_ss, h_rs, sa_ss, sa_rs, sb_ss, sb_rs, own_ss, fwd_ss, pf_ss, slg_rs,
    yo_ss, yo_rs, yv_ss, yv_rs, yg_ss, yg_rs, zo_ss, zo_rs, zv_ss, zv_rs, zg_ss, zg_rs, ty_ss, ty_rs, tz_ss, tz_rs,
):
    z, y, x, c = (lax.axis_index(a) for a in ("z", "y", "x", "c"))
    rows, D = xv.shape
    T = rows // S
    DB = D // 8
    DQ = DB // 4
    RB = D // (Z * Y)
    CH = rows // NC
    H = K - 1

    yn = (y + 1) % Y
    zn = (z + (y + 1) // Y) % Z
    yb = (y + Y - 1) % Y
    zb = (z + Z - 1 + (y + Y - 1) // Y) % Z
    first = (z + y) == 0
    last = (z * Y + y) == (Z * Y - 1)
    xp, xm = (x + 1) % 4, (x + 3) % 4
    xs = (x, x + 1 - 2 * (x % 2), (x + 2) % 4, 3 - x)
    cc = (c, 1 - c)

    def to(z=z, y=y, x=x, c=c):
        return {"z": z, "y": y, "x": x, "c": c}

    def remote(src, dst, ss, rs, dev):
        return pltpu.make_async_remote_copy(
            src_ref=src, dst_ref=dst, send_sem=ss, recv_sem=rs, device_id=dev, device_id_type=MESH
        )

    tp_peers = [to(x=xs[o // 2], c=cc[o % 2]) for o in range(1, 8)]
    y_peers = [to(y=(y + d) % Y) for d in range(1, Y)]
    z_peers = [to(z=(z + d) % Z) for d in range(1, Z)]
    nxt, prv = to(z=zn, y=yn), to(z=zb, y=yb)
    sent = []

    loads = [
        pltpu.make_async_copy(vp_hbm, wvg.at[:, pl.ds(0, L)], l_sem.at[0]),
        pltpu.make_async_copy(gp_hbm, wvg.at[:, pl.ds(L, L)], l_sem.at[1]),
        pltpu.make_async_copy(op_hbm, wo, l_sem.at[2]),
    ]
    loads[0].start()
    loads[1].start()
    XC = 4
    XR = rows // XC

    def x_load(i):
        at = pl.ds(pl.multiple_of(i * XR, XR), XR)
        return pltpu.make_async_copy(x_hbm.at[at], xv.at[at], x_sem.at[i])

    def g_load(i):
        at = pl.ds(pl.multiple_of(i * XR, XR), XR)
        return pltpu.make_async_copy(g_hbm.at[at], gv.at[at], g_sem.at[i])

    for i in (XC - 1, *range(XC - 1)):
        x_load(i).start()
    loads[2].start()
    for i in range(XC):
        g_load(i).start()

    barrier = pltpu.get_barrier_semaphore()
    greet = [*tp_peers, *y_peers, *z_peers, nxt, prv]
    for dev in greet:
        pl.semaphore_signal(barrier, inc=1, device_id=dev, device_id_type=MESH)

    loads[0].wait()
    loads[1].wait()

    def x_step(i, end):
        x_load(i).wait()
        res = dot_nn(xv[pl.ds(pl.multiple_of(i * XR, XR), XR), :], wvg[...])
        v = res[:, :L]
        s = jax.nn.sigmoid(res[:, L:])
        m = (v * s).astype(BF16).astype(F32)
        for h in range(XR // T):
            n = i * (XR // T) + h
            part = slice(h * T, (h + 1) * T)
            vbuf[pl.ds(n * NP, T), :] = v[part]
            sbuf[pl.ds(n * NP, T), :] = s[part]
            hist[pl.ds(n * HP + PAD, T), :] = m[part]
            if end and h == XR // T - 1:
                tail[...] = m[XR - PAD :]
            else:
                hist[pl.ds((n + 1) * HP, PAD), :] = m[(h + 1) * T - PAD : (h + 1) * T]

    x_step(XC - 1, True)

    def x_loop(i, carry):
        x_step(i, False)
        return carry

    lax.fori_loop(0, XC - 1, x_loop, 0)

    pl.semaphore_wait(barrier, len(greet))
    halo_m = remote(tail, halo_in, h_ss.at[0], h_rs.at[0], nxt)
    halo_m.start()

    yq, zq = y % 2, z % 2
    w_copies, w_own = [], []
    for o in range(1, 8):
        px, pc = xs[o // 2], cc[o % 2]
        row = (px * 2 + pc) * DB
        if o == 1:
            for i in range(4):
                at = pl.ds(pl.multiple_of(row + i * DQ, DQ), DQ)
                w_own.append(remote(wvg.at[at], wg.at[0, i // 2, i % 2], wo_ss.at[i], wo_rs.at[i], tp_peers[0]))
                w_own[-1].start()
        else:
            at = pl.ds(pl.multiple_of(row + (2 * yq + zq) * DQ, DQ), DQ)
            w_copies.append(
                remote(wvg.at[at], wg.at[o - 1, yq, zq], w_ss.at[o - 2], w_rs.at[o - 2], tp_peers[o - 1])
            )
            w_copies[-1].start()
    sent.extend([*w_own, *w_copies])

    loads[2].wait()

    def g_loop(i, carry):
        g_load(i).wait()
        r = dot_nn(gv[pl.ds(pl.multiple_of(i * XR, XR), XR), :], wo[...])
        for h in range(XR // T):
            slope[pl.ds((i * (XR // T) + h) * NP, T), :] = r[h * T : (h + 1) * T]
        return carry

    lax.fori_loop(0, XC, g_loop, 0)

    lane = lax.broadcasted_iota(jnp.int32, (S, L), 1)
    zero = jnp.zeros((S, L), F32)

    def near(ref, t):
        return ref[pl.ds(t, S, stride=NP), :]

    def wide(ref, t):
        return ref[pl.ds(t, S, stride=HP), :]

    def spread(stat, t):
        return jnp.sum(jnp.where(lane == t, stat, 0.0), axis=1, keepdims=True)

    def tap(k):
        return taps[pl.ds(k, 1), :]

    def conv_block(b, carry):
        s1, s2 = carry
        t0 = b * J
        r = [zero] * J
        for i in range(J + H):
            m = wide(hist, t0 + (PAD - H) + i)
            for j in range(J):
                k = H + j - i
                if 0 <= k < K:
                    r[j] = r[j] + tap(k) * m
        for j in range(J):
            convp[t0 + j] = r[j]
            s1 = jnp.where(lane == t0 + j, jnp.sum(r[j], axis=1, keepdims=True), s1)
            s2 = jnp.where(lane == t0 + j, jnp.sum(r[j] * r[j], axis=1, keepdims=True), s2)
        return s1, s2

    def exchange(own, got, ss, rs):
        copies = [remote(own, got.at[i], ss.at[i], rs.at[i], tp_peers[i]) for i in range(7)]
        for cp in copies:
            cp.start()
        sent.extend(copies)
        return copies

    def total(own, got, i):
        r = own[i]
        for p in range(7):
            r = r + got[p, i]
        return r * (1.0 / C)

    near_end = -(-H // J)
    s1, s2 = lax.fori_loop(near_end, T // J, conv_block, (zero, zero))
    halo_m.wait_recv()
    hist[pl.ds(0, PAD), :] = jnp.where(first, 0.0, halo_in[...])
    s1, s2 = lax.fori_loop(0, near_end, conv_block, (s1, s2))
    sta[0] = s1
    sta[1] = s2
    ex = exchange(sta, star, sa_ss, sa_rs)

    for cp in w_copies:
        cp.wait_recv()
    at = wg.at[pl.ds(1, 6), yq, zq]
    w_y = remote(at, at, wy_ss.at[0], wy_rs.at[0], to(y=y + 1 - 2 * yq))
    w_y.start()
    sent.append(w_y)

    for cp in ex:
        cp.wait_recv()
    center = total(sta, star, 0)
    inverse = lax.rsqrt(total(sta, star, 1) - center * center + norm_floor)
    gains = gain[...]

    def norm_block(b, carry):
        gsum, s1, s2 = carry
        t0 = b * J
        for j in range(J):
            t = t0 + j
            iv = jnp.broadcast_to(spread(inverse, t), (S, L))
            n = (convp[t] - spread(center, t)) * iv
            sc = n * gains
            sq = jax.nn.sigmoid(sc)
            act[pl.ds(t, S, stride=NP), :] = sc * sq
            ps = near(slope, t) * sq * (1.0 + sc * (1.0 - sq))
            gsum = gsum + ps * n
            ns = ps * gains
            inv[t] = iv
            nrm[t] = n
            nsl[t] = ns
            s1 = jnp.where(lane == t, jnp.sum(ns, axis=1, keepdims=True), s1)
            s2 = jnp.where(lane == t, jnp.sum(ns * n, axis=1, keepdims=True), s2)
        return gsum, s1, s2

    gsum, s1, s2 = lax.fori_loop(0, T // J, norm_block, (zero, zero, zero))
    stb[0] = s1
    stb[1] = s2
    ex = exchange(stb, stbr, sb_ss, sb_rs)

    at = wg.at[pl.ds(1, 6), 1 - yq, zq]
    remote(at, at, wy_ss.at[0], wy_rs.at[0], to(y=y + 1 - 2 * yq)).wait_recv()
    at = wg.at[pl.ds(1, 6), :, zq]
    w_z = remote(at, at, wy_ss.at[1], wy_rs.at[1], to(z=z + 1 - 2 * zq))
    w_z.start()
    sent.append(w_z)

    def flip(src, dst, row0):
        def step(n, carry):
            dst[pl.ds(row0, L), pl.ds(pl.multiple_of(n * T, T), T)] = src[pl.ds(n * NP, T), :].T.astype(BF16)
            return carry

        lax.fori_loop(0, S, step, 0)

    flip(act, actT, 0)

    def weight_block(left, right, zi, dsts):
        at = pl.ds(pl.multiple_of(zi * (D // Z), D // Z), D // Z)
        r = dot_nn(left[...], right[:, at]).T.astype(BF16)
        for n, dst in enumerate(dsts):
            for yi in range(Y):
                dst[zi, yi] = r[yi * RB : (yi + 1) * RB, n * L : (n + 1) * L]

    def y_send(src, dst, ss, rs):
        copies = []
        for d in range(1, Y):
            copies.append(
                remote(src.at[:, (y + d) % Y], dst.at[d - 1], ss.at[d - 1], rs.at[d - 1], y_peers[d - 1])
            )
            copies[-1].start()
        sent.extend(copies)
        return copies

    def out_loop(zi, carry):
        weight_block(actT, gv, zi, (wgo,))
        return carry

    lax.fori_loop(0, Z, out_loop, 0)

    for cp in ex:
        cp.wait_recv()
    slope_sum = total(stb, stbr, 0)
    cross_sum = total(stb, stbr, 1)

    def cs_block(b, carry):
        t0 = b * J
        for j in range(J):
            t = t0 + j
            cs[pl.ds(t, S, stride=HP), :] = inv[t] * (
                nsl[t] - spread(slope_sum, t) - nrm[t] * spread(cross_sum, t)
            )
        return carry

    lax.fori_loop(0, PAD // J, cs_block, 0)
    halo_out[...] = cs[pl.ds(0, PAD), :]
    halo_c = remote(halo_out, halo_back, h_ss.at[1], h_rs.at[1], prv)
    halo_c.start()
    yo = y_send(wgo, yro, yo_ss, yo_rs)
    for n in range(S - 1):
        cs[pl.ds(n * HP + T, PAD), :] = cs[pl.ds((n + 1) * HP, PAD), :]
    lax.fori_loop(PAD // J, T // J, cs_block, 0)

    def slope_block(b, carry):
        t0 = b * J
        r = [zero] * J
        for i in range(J + H):
            f = wide(cs, t0 + i)
            for j in range(J):
                k = i - j
                if 0 <= k < K:
                    r[j] = r[j] + tap(k) * f
        for j in range(J):
            t = t0 + j
            s = near(sbuf, t)
            rs = r[j] * s
            vsf[pl.ds(t, S, stride=NP), :] = rs
            gsf[pl.ds(t, S, stride=NP), :] = rs * near(vbuf, t) * (1.0 - s)
        return carry

    free = (T - H) // J
    lax.fori_loop(0, free, slope_block, 0)

    def tap_block(b, sums):
        sums = list(sums)
        t0 = b * 8
        e = [wide(cs, t0 + j) for j in range(8)]
        for i in range(8 + H):
            m = wide(hist, t0 + (PAD - H) + i)
            for j in range(8):
                k = H + j - i
                if 0 <= k < K:
                    sums[k] = sums[k] + e[j] * m
        return tuple(sums)

    sums = lax.fori_loop(0, T // 8, tap_block, tuple(zero for _ in range(K)))
    for k in range(K):
        tgs[pl.ds(k, 1), :] = jnp.sum(sums[k], axis=0, keepdims=True)
    tgs[pl.ds(K, 1), :] = jnp.sum(gsum, axis=0, keepdims=True)
    ty = []
    for d in range(1, Y):
        ty.append(remote(tgs, tgy.at[y], ty_ss.at[d - 1], ty_rs.at[d - 1], y_peers[d - 1]))
        ty[-1].start()
    sent.extend(ty)
    tgy[y] = tgs[...]

    halo_c.wait_recv()
    cs[pl.ds((S - 1) * HP + T, PAD), :] = jnp.where(last, 0.0, halo_back[...])
    lax.fori_loop(free, T // J, slope_block, 0)

    def to_bf16(n, carry):
        at = pl.ds(pl.multiple_of(n * T, T), T)
        sl[at, pl.ds(0, L)] = vsf[pl.ds(n * NP, T), :].astype(BF16)
        sl[at, pl.ds(L, L)] = gsf[pl.ds(n * NP, T), :].astype(BF16)
        return carry

    lax.fori_loop(0, S, to_bf16, 0)

    def piece(ref, q):
        return ref.at[pl.ds(q * CH, CH)]

    def own_copy(way, slot, q, dev):
        return remote(piece(sl, q), piece(slg.at[slot], q), own_ss.at[way, q], slg_rs.at[slot, q], dev)

    right, left = to(x=xp), to(x=xm)
    partner = to(c=1 - c)
    up = [own_copy(0, 1, q, right) for q in range(NC)]
    down = [own_copy(1, 2, q, left) for q in range(NC)]
    over = [own_copy(2, 0, q, partner) for q in range(NC)]
    half = NC // 2
    for i in range(NC):
        up[i].start()
        down[(i + half) % NC].start()
    for i in range(NC):
        over[i].start()
    sent.extend([*up, *down, *over])

    flip(vsf, slT, 0)
    flip(gsf, slT, L)

    def gate_send(d):
        return remote(
            wgg.at[(z + 1 + d) % Z], zrg.at[d], zg_ss.at[d], zg_rs.at[d], to(z=(z + 1 + d) % Z)
        )

    def vg_loop(d, carry):
        weight_block(slT, xv, (z + 1 + d) % Z, (wgv, wgg))
        gate_send(d).start()
        return carry

    lax.fori_loop(0, Z - 1, vg_loop, 0)
    weight_block(slT, xv, z, (wgv, wgg))
    yv = y_send(wgv, yrv, yv_ss, yv_rs)
    zg = [gate_send(d) for d in range(Z - 1)]
    sent.extend(zg)

    for cp in w_own:
        cp.wait_recv()
    at = wg.at[pl.ds(1, 6), :, 1 - zq]
    remote(at, at, wy_ss.at[1], wy_rs.at[1], to(z=z + 1 - 2 * zq)).wait_recv()

    def weights_from(slot):
        core = 1 if slot == 0 or slot > 3 else 0
        base = slot if slot <= 3 else slot - 3
        if base == 0:
            return wg[0].reshape(DB, 2 * L)
        if base == 3:
            return wg[3 + core].reshape(DB, 2 * L)
        way = 3 - 2 * (x % 2) if base == 1 else 1 + 2 * (x % 2)
        return wg[2 * way + core - 1].reshape(DB, 2 * L)

    at = pl.ds(pl.multiple_of((x * 2 + c) * DB, DB), DB)
    acc[...] = dot_nt(sl[...], wvg[at, :])

    def add(slot, q):
        at = pl.ds(q * CH, CH)
        acc[at, :] += dot_nt(slg[slot, at, :], weights_from(slot))

    def pf(slot, q):
        cp = remote(
            piece(slg.at[slot], q), piece(slg.at[slot + 3], q), pf_ss.at[slot - 1, q], slg_rs.at[slot + 3, q], partner
        )
        cp.start()
        sent.append(cp)
        return cp

    fwd = {}
    pfs = {}
    for i in range(NC):
        q = i
        up[q].wait_recv()
        if i < half:
            fwd[q] = remote(piece(slg.at[1], q), piece(slg.at[3], q), fwd_ss.at[q], slg_rs.at[3, q], right)
            fwd[q].start()
        pfs[1, q] = pf(1, q)
        q2 = (i + half) % NC
        down[q2].wait_recv()
        if i < half:
            fwd[q2] = remote(piece(slg.at[2], q2), piece(slg.at[3], q2), fwd_ss.at[q2], slg_rs.at[3, q2], left)
            fwd[q2].start()
        pfs[2, q2] = pf(2, q2)
        over[i].wait_recv()
        add(0, i)
        add(1, q)
        add(2, q2)
        if i == half:
            for cp in yo:
                cp.wait_recv()
            zo = second(Z, Y, y, z, wgo, yro, zso, zro, zo_ss, zo_rs, z_peers, remote, sent)
            for cp in ty:
                cp.wait_recv()
            t = tgy[0]
            for yi in range(1, Y):
                t = t + tgy[yi]
            tgzs[...] = t
            tgz[z] = t
            tz = []
            for d in range(1, Z):
                tz.append(remote(tgzs, tgz.at[z], tz_ss.at[d - 1], tz_rs.at[d - 1], z_peers[d - 1]))
                tz[-1].start()
            sent.extend(tz)
    sent.extend(fwd.values())
    for q in range(NC):
        pfs[1, q].wait_recv()
        add(4, q)
        pfs[2, q].wait_recv()
        add(5, q)

    for cp in yv:
        cp.wait_recv()
    zv = second(Z, Y, y, z, wgv, yrv, zsv, zrv, zv_ss, zv_rs, z_peers, remote, sent)
    for cp in zg:
        cp.wait_recv()
    for yi in range(Y):
        r = wgg[z, yi].astype(F32)
        for d in range(Z - 1):
            r = r + zrg[d, yi].astype(F32)
        ysg[yi] = r.astype(BF16)
    yg = []
    for d in range(1, Y):
        yg.append(remote(ysg.at[(y + d) % Y], yrg.at[d - 1], yg_ss.at[d - 1], yg_rs.at[d - 1], y_peers[d - 1]))
        yg[-1].start()
    sent.extend(yg)

    order = [q for i in range(half) for q in (i, i + half)]
    for q in order:
        fwd[q].wait_recv()
        pfs[3, q] = pf(3, q)
        add(3, q)
    for q in order:
        pfs[3, q].wait_recv()
        add(6, q)
    ig[...] = acc[...].astype(BF16)

    def finish(copies, own, got, count):
        for cp in copies:
            cp.wait_recv()
        r = own.astype(F32)
        for d in range(count - 1):
            r = r + got[d].astype(F32)
        return r

    og[...] = finish(zo, zso[z], zro, Z)
    for cp in tz:
        cp.wait_recv()
    t = tgz[0]
    for zi in range(1, Z):
        t = t + tgz[zi]
    tg[...] = t[:K]
    ng[...] = t[K : K + 1]
    vg[...] = finish(zv, zsv[z], zrv, Z)
    gg[...] = finish(yg, ysg[y], yrg, Y)

    for cp in [halo_m, halo_c, *sent]:
        cp.wait_send()


def second(Z, Y, y, z, own, got, zs, zr, ss, rs, z_peers, remote, sent):
    def step(zi, carry):
        r = own[zi, y].astype(F32)
        for d in range(Y - 1):
            r = r + got[d, zi].astype(F32)
        zs[zi] = r.astype(BF16)
        return carry

    lax.fori_loop(0, Z, step, 0)
    copies = []
    for d in range(1, Z):
        copies.append(remote(zs.at[(z + d) % Z], zr.at[d - 1], ss.at[d - 1], rs.at[d - 1], z_peers[d - 1]))
        copies[-1].start()
    sent.extend(copies)
    return copies


def write_out(*refs):
    half = len(refs) // 2
    for src, dst in zip(refs[:half], refs[half:]):
        dst[...] = src[...]


def shards(Z, Y, block_input, value_proj, gate_proj, conv_taps, norm_gain, out_proj, grad_output):
    rows, D = block_input.shape
    K = conv_taps.shape[0]
    C = value_proj.shape[1] * 8
    DB, RB, T = D // 8, D // (Z * Y), rows // S
    vm = pltpu.VMEM
    dma = pltpu.SemaphoreType.DMA
    hbm, vmem = pl.BlockSpec(memory_space=ANYWHERE), pl.BlockSpec(memory_space=pltpu.VMEM)
    near, wide = vm((S * NP, L), F32), vm((S * HP, L), F32)
    flat = vm((T, S, L), F32)
    halo = vm((PAD, L), F32)
    stat, stats = vm((2, S, L), F32), vm((7, 2, S, L), F32)
    scratch = [
        vm((rows, D), BF16), vm((rows, D), BF16), vm((D, 2 * L), BF16), vm((D, L), BF16), vm((7, 2, 2, DB // 4, 2 * L), BF16),
        near, near, near, wide, flat, flat, flat, flat, near, wide,
        near, near, vm((rows, 2 * L), BF16), vm((7, rows, 2 * L), BF16), vm((rows, DB), F32),
        halo, halo, halo, halo,
        vm((L, rows), BF16), vm((2 * L, rows), BF16),
        *[vm((Z, Y, RB, L), BF16) for _ in range(3)],
        vm((Y - 1, Z, RB, L), BF16), vm((Y - 1, Z, RB, L), BF16),
        vm((Z, RB, L), BF16), vm((Z, RB, L), BF16), vm((Z - 1, RB, L), BF16), vm((Z - 1, RB, L), BF16),
        vm((Z - 1, Y, RB, L), BF16), vm((Y, RB, L), BF16), vm((Y - 1, RB, L), BF16),
        stat, stats, stat, stats,
        halo, vm((Y, PAD, L), F32), halo, vm((Z, PAD, L), F32),
        dma((3,)), dma((4,)), dma((4,)), dma((4,)), dma((4,)), dma((6,)), dma((6,)), dma((2,)), dma((2,)), dma((2,)), dma((2,)),
        dma((7,)), dma((7,)), dma((7,)), dma((7,)), dma((3, NC)), dma((NC,)), dma((3, NC)), dma((7, NC)),
        *[dma((Y - 1,)) for _ in range(6)], *[dma((Z - 1,)) for _ in range(6)],
        dma((Y - 1,)), dma((Y - 1,)), dma((Z - 1,)), dma((Z - 1,)),
    ]
    shapes = (
        jax.ShapeDtypeStruct((rows, DB), BF16),
        jax.ShapeDtypeStruct((RB, L), F32),
        jax.ShapeDtypeStruct((RB, L), F32),
        jax.ShapeDtypeStruct((RB, L), F32),
        jax.ShapeDtypeStruct((K, L), F32),
        jax.ShapeDtypeStruct((1, L), F32),
    )
    block_input, value_proj, gate_proj, out_proj, grad_output = (
        pltpu.with_memory_space_constraint(a, pltpu.HBM)
        for a in (block_input, value_proj, gate_proj, out_proj, grad_output)
    )
    outs = pl.pallas_call(
        functools.partial(body, Z, Y, C, K),
        out_shape=shapes,
        in_specs=[hbm, hbm, hbm, vmem, vmem, hbm, hbm],
        out_specs=[vmem] * 6,
        scratch_shapes=scratch,
        compiler_params=pltpu.CompilerParams(
            collective_id=0, has_side_effects=True, vmem_limit_bytes=VMEM_LIMIT
        ),
        name="block_backward",
    )(block_input, value_proj, gate_proj, conv_taps, norm_gain.reshape(1, L), out_proj, grad_output)
    outs = pl.pallas_call(
        write_out,
        out_shape=shapes,
        in_specs=[vmem] * 6,
        out_specs=[vmem] * 6,
        compiler_params=pltpu.CompilerParams(vmem_limit_bytes=4 * 1024 * 1024),
        name="write_out",
    )(*outs)
    return (*outs[:5], outs[5].reshape(L))


def solution(mesh):
    tp = mesh.shape["tp"]
    Y = 4
    Z = mesh.shape["sp"] // Y
    finer = Mesh(mesh.devices.reshape(Z, Y, tp // 2, 2), ("z", "y", "x", "c"))
    sp, ch = ("z", "y"), ("x", "c")
    return jax.shard_map(
        functools.partial(shards, Z, Y),
        mesh=finer,
        in_specs=(P(sp, None), P(None, ch), P(None, ch), P(None, ch), P(ch), P(None, ch), P(sp, None)),
        out_specs=(P(sp, ch), P(sp, ch), P(sp, ch), P(sp, ch), P(None, ch), P(ch)),
        check_vma=False,
    )
```

time: 79.4 us -> 60.5 us (0.76)
  Pallas kernels: 69.4 us -> 58.3 us
  local copies, waits for them, and re-layouts: 8.43 us -> 1.37 us
    pallas_call x1 -> x2, Pallas kernels: 69.4 us -> 58.3 us  [the longest x1 57.5 us: shards(): pl.pallas_call(functools.partial(body, Z, Y, C, K), out_shape=shapes, in_...]
    unnamed x6 -> x4, local copies, waits for them, and re-layouts: 8.43 us -> 1.37 us
where the time goes in v2:
time: 60.5 us; the launch traced here: 60.4 us
  Pallas kernels  58.3 us (96%)
  local copies, waits for them, and re-layouts  1.37 us (2%)
  between operations  0.65 us (1%)
    pallas_call x1, Pallas kernels, shards(): pl.pallas_call(functools.partial(body, Z, Y, C, K), out_shape=shapes, in_...  57.5 us
    unnamed x4, local copies, waits for them, and re-layouts  1.37 us

profile of v2, /device:TPU:2, one launch (start us, length us, event | category | flops | bytes accessed | tf_op | source)
XLA Modules:
  0.0 60.4 jit_solution(191560153168435362)
XLA Ops:
  0.6 0.0 copy-start
  0.6 0.7 %copy-done = f32[31,128]{1,0:T(8,128)S(1)} copy-done((f32[31,128]{1,0:T(8,128)S(1)}, f32[31,128]{1,0:T(8,128)}, u32[]{:S(2)}) %copy-start) | copy-done | bytes 15896
  1.4 0.0 copy-start.1
  1.4 0.7 %copy-done.1 = f32[128]{0:T(128)S(1)} copy-done((f32[128]{0:T(128)S(1)}, f32[128]{0:T(128)}, u32[]{:S(2)}) %copy-start.1) | copy-done | bytes 536
  2.0 57.5 %block_backward.1 = (bf16[1024,256]{1,0:T(8,128)(2,1)S(1)}, f32[64,128]{1,0:T(8,128)S(1)}, f32[64,128]{1,0:T(8,128)S(1)}, f32[64,128]{1,0:T(8,128)S(1)}, f32[31,128]{1,0:T(8,128)S(1)}, /*index=5*/f32[1,128]{1,0:T(1,128)S(1)}) custom-call(bf16[1024,2048]{1,0:T(8,128)(2,1)} %x_hbm.1, bf16[2048,128]{1,0:T(8,128)(2,1)} %vp_hbm.1, bf16[2048,128]{1,0:T(8,128)(2,1)} %gp_hbm.1, ...), custom_call_target="tpu_custom_call" | custom-call | tf_op jit(solution)/shard_map/block_backward/pallas_call | solution.py:598
  59.5 0.9 %write_out.1 = (bf16[1024,256]{1,0:T(8,128)(2,1)}, f32[64,128]{1,0:T(8,128)}, f32[64,128]{1,0:T(8,128)}, f32[64,128]{1,0:T(8,128)}, f32[31,128]{1,0:T(8,128)}, /*index=5*/f32[1,128]{1,0:T(1,128)}) custom-call(bf16[1024,256]{1,0:T(8,128)(2,1)S(1)} %get-tuple-element.18.refs_0_, f32[64,128]{1,0:T(8,128)S(1)} %get-tuple-element.19.refs_1_, ...), custom_call_target="tpu_custom_call" | custom-call | tf_op jit(solution)/shard_map/write_out/pallas_call | solution.py:609
Async XLA Ops:
  0.6 0.7 %copy-start = (f32[31,128]{1,0:T(8,128)S(1)}, f32[31,128]{1,0:T(8,128)}, u32[]{:S(2)}) copy-start(f32[31,128]{1,0:T(8,128)} %taps.1) | copy-start | bytes 47620
  1.4 0.7 %copy-start.1 = (f32[128]{0:T(128)S(1)}, f32[128]{0:T(128)}, u32[]{:S(2)}) copy-start(f32[128]{0:T(128)} %param.11) | copy-start | bytes 1540

commit v3 on v2

--- a/solution.py
+++ b/solution.py
@@ -20,6 +20,8 @@
 NP = 132
 HP = 164
 PAD = 32
+NN = 4
+FAR0, NF = 3, 3
 NC = 4
 
 
@@ -33,13 +35,14 @@
 
 def body(
     Z, Y, C, K,
-    x_hbm, vp_hbm, gp_hbm, taps, gain, op_hbm, g_hbm,
+    x_hbm, vp_hbm, gp_hbm, taps_hbm, gain_hbm, op_hbm, g_hbm,
     ig, vg, gg, og, tg, ng,
     xv, gv, wvg, wo, wg, vbuf, sbuf, slope, hist, convp, nrm, nsl, inv, act, cs, vsf, gsf, sl, slg, acc,
-    tail, halo_in, halo_out, halo_back,
-    actT, slT, wgo, wgv, wgg, yro, yrv, zso, zsv, zro, zrv, zrg, ysg, yrg, sta, star, stb, stbr, tgs, tgy, tgzs, tgz,
-    l_sem, x_sem, g_sem, wo_ss, wo_rs, w_ss, w_rs, wy_ss, wy_rs, h_ss, h_rs, sa_ss, sa_rs, sb_ss, sb_rs, own_ss, fwd_ss, pf_ss, slg_rs,
-    yo_ss, yo_rs, yv_ss, yv_rs, yg_ss, yg_rs, zo_ss, zo_rs, zv_ss, zv_rs, zg_ss, zg_rs, ty_ss, ty_rs, tz_ss, tz_rs,
+    tail, halo_in, halo_out, halo_back, taps, gain,
+    actT, slT, wgo, wvf, wvn, wgn, yro, yrf, yrv, zso, zsf, zsv, zro, zrf, zrv, zrg, ysg, yrg, sta, star, stb, stbr, tgs, tgy, tgzs, tgz,
+    in_sem, l_sem, x_sem, g_sem, wo_ss, wo_rs, w_ss, w_rs, wy_ss, wy_rs, h_ss, h_rs, sa_ss, sa_rs, sb_ss, sb_rs, own_ss, fwd_ss, pf_ss, slg_rs,
+    yo_ss, yo_rs, yf_ss, yf_rs, yv_ss, yv_rs, yg_ss, yg_rs, zo_ss, zo_rs, zf_ss, zf_rs, zv_ss, zv_rs, zg_ss, zg_rs,
+    ty_ss, ty_rs, tz_ss, tz_rs,
 ):
     z, y, x, c = (lax.axis_index(a) for a in ("z", "y", "x", "c"))
     rows, D = xv.shape
@@ -78,6 +81,8 @@
         pltpu.make_async_copy(vp_hbm, wvg.at[:, pl.ds(0, L)], l_sem.at[0]),
         pltpu.make_async_copy(gp_hbm, wvg.at[:, pl.ds(L, L)], l_sem.at[1]),
         pltpu.make_async_copy(op_hbm, wo, l_sem.at[2]),
+        pltpu.make_async_copy(taps_hbm, taps, l_sem.at[3]),
+        pltpu.make_async_copy(gain_hbm, gain, l_sem.at[4]),
     ]
     loads[0].start()
     loads[1].start()
@@ -94,14 +99,47 @@
 
     for i in (XC - 1, *range(XC - 1)):
         x_load(i).start()
-    loads[2].start()
+    for cp in loads[2:]:
+        cp.start()
     for i in range(XC):
         g_load(i).start()
 
     barrier = pltpu.get_barrier_semaphore()
-    greet = [*tp_peers, *y_peers, *z_peers, nxt, prv]
-    for dev in greet:
+    for dev in (*tp_peers, *y_peers):
         pl.semaphore_signal(barrier, inc=1, device_id=dev, device_id_type=MESH)
+    below, above = z > 0, z < Z - 1
+    into, out_of = (y == 0) & below, (y == Y - 1) & above
+    for there, dev in (
+        (below, to(z=(z + Z - 1) % Z)),
+        (above, to(z=(z + 1) % Z)),
+        (into, prv),
+        (out_of, nxt),
+    ):
+
+        @pl.when(there)
+        def _(dev=dev):
+            pl.semaphore_signal(barrier, inc=1, device_id=dev, device_id_type=MESH)
+
+    greeted = len(tp_peers) + len(y_peers) + sum(
+        jnp.where(there, 1, 0) for there in (below, above, into, out_of)
+    )
+
+    def pass_on(k):
+        n = 2**k
+        for i, there, at in ((0, z + n < Z, (z + n) % Z), (1, z >= n, (z + Z - n) % Z)):
+
+            @pl.when(there)
+            def _(i=i, at=at):
+                pl.semaphore_signal(in_sem.at[2 * k + i], inc=1, device_id=to(z=at), device_id_type=MESH)
+
+    def heard(k):
+        n = 2**k
+        for i, there in ((0, z >= n), (1, z + n < Z)):
+
+            @pl.when(there)
+            def _(i=i):
+                pl.semaphore_wait(in_sem.at[2 * k + i], 1)
+
 
     loads[0].wait()
     loads[1].wait()
@@ -129,11 +167,16 @@
         x_step(i, False)
         return carry
 
-    lax.fori_loop(0, XC - 1, x_loop, 0)
-
-    pl.semaphore_wait(barrier, len(greet))
+    x_step(0, False)
+
+    pl.semaphore_wait(barrier, greeted)
     halo_m = remote(tail, halo_in, h_ss.at[0], h_rs.at[0], nxt)
-    halo_m.start()
+
+    @pl.when(jnp.logical_not(last))
+    def _():
+        halo_m.start()
+
+    pass_on(0)
 
     yq, zq = y % 2, z % 2
     w_copies, w_own = [], []
@@ -153,7 +196,10 @@
             w_copies[-1].start()
     sent.extend([*w_own, *w_copies])
 
-    loads[2].wait()
+    lax.fori_loop(1, XC - 1, x_loop, 0)
+
+    for cp in loads[2:]:
+        cp.wait()
 
     def g_loop(i, carry):
         g_load(i).wait()
@@ -210,8 +256,16 @@
 
     near_end = -(-H // J)
     s1, s2 = lax.fori_loop(near_end, T // J, conv_block, (zero, zero))
-    halo_m.wait_recv()
-    hist[pl.ds(0, PAD), :] = jnp.where(first, 0.0, halo_in[...])
+
+    @pl.when(first)
+    def _():
+        hist[pl.ds(0, PAD), :] = jnp.zeros((PAD, L), F32)
+
+    @pl.when(jnp.logical_not(first))
+    def _():
+        halo_m.wait_recv()
+        hist[pl.ds(0, PAD), :] = halo_in[...]
+
     s1, s2 = lax.fori_loop(0, near_end, conv_block, (s1, s2))
     sta[0] = s1
     sta[1] = s2
@@ -220,9 +274,15 @@
     for cp in w_copies:
         cp.wait_recv()
     at = wg.at[pl.ds(1, 6), yq, zq]
-    w_y = remote(at, at, wy_ss.at[0], wy_rs.at[0], to(y=y + 1 - 2 * yq))
-    w_y.start()
-    sent.append(w_y)
+    w_on = [
+        remote(at, at, wy_ss.at[0], wy_rs.at[0], to(y=y + 1 - 2 * yq)),
+        remote(at, at, wy_ss.at[1], wy_rs.at[1], to(z=z + 1 - 2 * zq)),
+    ]
+    for cp in w_on:
+        cp.start()
+    sent.extend(w_on)
+    heard(0)
+    pass_on(1)
 
     for cp in ex:
         cp.wait_recv()
@@ -254,13 +314,8 @@
     stb[0] = s1
     stb[1] = s2
     ex = exchange(stb, stbr, sb_ss, sb_rs)
-
-    at = wg.at[pl.ds(1, 6), 1 - yq, zq]
-    remote(at, at, wy_ss.at[0], wy_rs.at[0], to(y=y + 1 - 2 * yq)).wait_recv()
-    at = wg.at[pl.ds(1, 6), :, zq]
-    w_z = remote(at, at, wy_ss.at[1], wy_rs.at[1], to(z=z + 1 - 2 * zq))
-    w_z.start()
-    sent.append(w_z)
+    heard(1)
+    pass_on(2)
 
     def flip(src, dst, row0):
         def step(n, carry):
@@ -271,12 +326,11 @@
 
     flip(act, actT, 0)
 
-    def weight_block(left, right, zi, dsts):
+    def weight_block(left, right, zi, put):
         at = pl.ds(pl.multiple_of(zi * (D // Z), D // Z), D // Z)
         r = dot_nn(left[...], right[:, at]).T.astype(BF16)
-        for n, dst in enumerate(dsts):
-            for yi in range(Y):
-                dst[zi, yi] = r[yi * RB : (yi + 1) * RB, n * L : (n + 1) * L]
+        for yi in range(Y):
+            put(yi, r[yi * RB : (yi + 1) * RB])
 
     def y_send(src, dst, ss, rs):
         copies = []
@@ -289,7 +343,10 @@
         return copies
 
     def out_loop(zi, carry):
-        weight_block(actT, gv, zi, (wgo,))
+        def put(yi, r):
+            wgo[zi, yi] = r
+
+        weight_block(actT, gv, zi, put)
         return carry
 
     lax.fori_loop(0, Z, out_loop, 0)
@@ -311,7 +368,16 @@
     lax.fori_loop(0, PAD // J, cs_block, 0)
     halo_out[...] = cs[pl.ds(0, PAD), :]
     halo_c = remote(halo_out, halo_back, h_ss.at[1], h_rs.at[1], prv)
-    halo_c.start()
+
+    @pl.when(jnp.logical_not(first))
+    def _():
+        halo_c.start()
+
+    at = wg.at[pl.ds(1, 6), 1 - yq, zq]
+    remote(at, at, wy_ss.at[0], wy_rs.at[0], to(y=y + 1 - 2 * yq)).wait_recv()
+    w_z = remote(at, at, wy_ss.at[2], wy_rs.at[2], to(z=z + 1 - 2 * zq))
+    w_z.start()
+    sent.append(w_z)
     yo = y_send(wgo, yro, yo_ss, yo_rs)
     for n in range(S - 1):
         cs[pl.ds(n * HP + T, PAD), :] = cs[pl.ds((n + 1) * HP, PAD), :]
@@ -360,8 +426,16 @@
     sent.extend(ty)
     tgy[y] = tgs[...]
 
-    halo_c.wait_recv()
-    cs[pl.ds((S - 1) * HP + T, PAD), :] = jnp.where(last, 0.0, halo_back[...])
+
+    @pl.when(last)
+    def _():
+        cs[pl.ds((S - 1) * HP + T, PAD), :] = jnp.zeros((PAD, L), F32)
+
+    @pl.when(jnp.logical_not(last))
+    def _():
+        halo_c.wait_recv()
+        cs[pl.ds((S - 1) * HP + T, PAD), :] = halo_back[...]
+
     lax.fori_loop(free, T // J, slope_block, 0)
 
     def to_bf16(n, carry):
@@ -394,26 +468,46 @@
     flip(vsf, slT, 0)
     flip(gsf, slT, L)
 
-    def gate_send(d):
-        return remote(
-            wgg.at[(z + 1 + d) % Z], zrg.at[d], zg_ss.at[d], zg_rs.at[d], to(z=(z + 1 + d) % Z)
-        )
-
-    def vg_loop(d, carry):
-        weight_block(slT, xv, (z + 1 + d) % Z, (wgv, wgg))
-        gate_send(d).start()
-        return carry
-
-    lax.fori_loop(0, Z - 1, vg_loop, 0)
-    weight_block(slT, xv, z, (wgv, wgg))
-    yv = y_send(wgv, yrv, yv_ss, yv_rs)
-    zg = [gate_send(d) for d in range(Z - 1)]
+    def far_loop(e, carry):
+        def put(yi, r):
+            wvf[e, yi] = r
+
+        weight_block(slT, xv, (z + FAR0 + e) % Z, put)
+        return carry
+
+    def near_of(e):
+        return (z + Z + (1 + e // 2) * (1 - 2 * (e % 2))) % Z
+
+    def near_from(e):
+        return (z + Z - (1 + e // 2) * (1 - 2 * (e % 2))) % Z
+
+    def gate_send(e):
+        return remote(wgn.at[e], zrg.at[e], zg_ss.at[e], zg_rs.at[e], to(z=near_of(e)))
+
+    def near_put(e):
+        def put(yi, r):
+            wvn[e, yi] = r[:, :L]
+            wgn[e, yi] = r[:, L:]
+
+        return put
+
+    def near_loop(e, carry):
+        weight_block(slT, xv, near_of(e), near_put(e))
+        gate_send(e).start()
+        return carry
+
+    heard(2)
+    lax.fori_loop(0, NF, far_loop, 0)
+    yf = y_send(wvf, yrf, yf_ss, yf_rs)
+    lax.fori_loop(0, NN, near_loop, 0)
+    weight_block(slT, xv, z, near_put(NN))
+    yv = y_send(wvn, yrv, yv_ss, yv_rs)
+    zg = [gate_send(e) for e in range(NN)]
     sent.extend(zg)
 
-    for cp in w_own:
+    for cp in yo:
         cp.wait_recv()
-    at = wg.at[pl.ds(1, 6), :, 1 - zq]
-    remote(at, at, wy_ss.at[1], wy_rs.at[1], to(z=z + 1 - 2 * zq)).wait_recv()
+    zo = second(Z, Y, y, z, wgo, yro, zso, zro, zo_ss, zo_rs, z_peers, remote, sent)
 
     def weights_from(slot):
         core = 1 if slot == 0 or slot > 3 else 0
@@ -456,13 +550,17 @@
             fwd[q2].start()
         pfs[2, q2] = pf(2, q2)
         over[i].wait_recv()
-        add(0, i)
-        add(1, q)
-        add(2, q2)
-        if i == half:
-            for cp in yo:
+        if i == 1:
+            for cp in w_own:
                 cp.wait_recv()
-            zo = second(Z, Y, y, z, wgo, yro, zso, zro, zo_ss, zo_rs, z_peers, remote, sent)
+            for k, yi in ((1, yq), (2, 1 - yq)):
+                at = wg.at[pl.ds(1, 6), yi, 1 - zq]
+                remote(at, at, wy_ss.at[k], wy_rs.at[k], to(z=z + 1 - 2 * zq)).wait_recv()
+        for j in {0: (), 1: (0, 1)}.get(i, (i,)):
+            add(0, j)
+            add(1, j)
+            add(2, (j + half) % NC)
+        if i == 1:
             for cp in ty:
                 cp.wait_recv()
             t = tgy[0]
@@ -475,28 +573,51 @@
                 tz.append(remote(tgzs, tgz.at[z], tz_ss.at[d - 1], tz_rs.at[d - 1], z_peers[d - 1]))
                 tz[-1].start()
             sent.extend(tz)
+        if i == 2:
+            for cp in yf:
+                cp.wait_recv()
+            zf = []
+            for e in range(NF):
+                r = wvf[e, y].astype(F32)
+                for d in range(Y - 1):
+                    r = r + yrf[d, e].astype(F32)
+                zsf[e] = r.astype(BF16)
+                zf.append(remote(zsf.at[e], zrf.at[e], zf_ss.at[e], zf_rs.at[e], to(z=(z + FAR0 + e) % Z)))
+                zf[-1].start()
+            sent.extend(zf)
+            for cp in zg:
+                cp.wait_recv()
+            for yi in range(Y):
+                r = wgn[NN, yi].astype(F32)
+                for e in range(NN):
+                    r = r + zrg[e, yi].astype(F32)
+                ysg[yi] = r.astype(BF16)
+            yg = []
+            for d in range(1, Y):
+                yg.append(
+                    remote(ysg.at[(y + d) % Y], yrg.at[d - 1], yg_ss.at[d - 1], yg_rs.at[d - 1], y_peers[d - 1])
+                )
+                yg[-1].start()
+            sent.extend(yg)
+        if i == 3:
+            for cp in yv:
+                cp.wait_recv()
+            zv = []
+            for e in range(NN + 1):
+                r = wvn[e, y].astype(F32)
+                for d in range(Y - 1):
+                    r = r + yrv[d, e].astype(F32)
+                zsv[e] = r.astype(BF16)
+                if e < NN:
+                    zv.append(remote(zsv.at[e], zrv.at[e], zv_ss.at[e], zv_rs.at[e], to(z=near_of(e))))
+                    zv[-1].start()
+            sent.extend(zv)
     sent.extend(fwd.values())
     for q in range(NC):
         pfs[1, q].wait_recv()
         add(4, q)
         pfs[2, q].wait_recv()
         add(5, q)
-
-    for cp in yv:
-        cp.wait_recv()
-    zv = second(Z, Y, y, z, wgv, yrv, zsv, zrv, zv_ss, zv_rs, z_peers, remote, sent)
-    for cp in zg:
-        cp.wait_recv()
-    for yi in range(Y):
-        r = wgg[z, yi].astype(F32)
-        for d in range(Z - 1):
-            r = r + zrg[d, yi].astype(F32)
-        ysg[yi] = r.astype(BF16)
-    yg = []
-    for d in range(1, Y):
-        yg.append(remote(ysg.at[(y + d) % Y], yrg.at[d - 1], yg_ss.at[d - 1], yg_rs.at[d - 1], y_peers[d - 1]))
-        yg[-1].start()
-    sent.extend(yg)
 
     order = [q for i in range(half) for q in (i, i + half)]
     for q in order:
@@ -524,11 +645,30 @@
         t = t + tgz[zi]
     tg[...] = t[:K]
     ng[...] = t[K : K + 1]
-    vg[...] = finish(zv, zsv[z], zrv, Z)
-    gg[...] = finish(yg, ysg[y], yrg, Y)
-
-    for cp in [halo_m, halo_c, *sent]:
+    for cp in [*zf, *zv, *yg]:
+        cp.wait_recv()
+    far = zrf[0].astype(F32)
+    for e in range(1, NF):
+        far = far + zrf[e].astype(F32)
+    r = far[:, :L] + zsv[NN].astype(F32)
+    for e in range(NN):
+        r = r + zrv[e].astype(F32)
+    vg[...] = r
+    r = far[:, L:] + ysg[y].astype(F32)
+    for d in range(Y - 1):
+        r = r + yrg[d].astype(F32)
+    gg[...] = r
+
+    for cp in sent:
         cp.wait_send()
+
+    @pl.when(jnp.logical_not(last))
+    def _():
+        halo_m.wait_send()
+
+    @pl.when(jnp.logical_not(first))
+    def _():
+        halo_c.wait_send()
 
 
 def second(Z, Y, y, z, own, got, zs, zr, ss, rs, z_peers, remote, sent):
@@ -570,17 +710,19 @@
         vm((rows, D), BF16), vm((rows, D), BF16), vm((D, 2 * L), BF16), vm((D, L), BF16), vm((7, 2, 2, DB // 4, 2 * L), BF16),
         near, near, near, wide, flat, flat, flat, flat, near, wide,
         near, near, vm((rows, 2 * L), BF16), vm((7, rows, 2 * L), BF16), vm((rows, DB), F32),
-        halo, halo, halo, halo,
+        halo, halo, halo, halo, vm((K, L), F32), vm((1, L), F32),
         vm((L, rows), BF16), vm((2 * L, rows), BF16),
-        *[vm((Z, Y, RB, L), BF16) for _ in range(3)],
-        vm((Y - 1, Z, RB, L), BF16), vm((Y - 1, Z, RB, L), BF16),
-        vm((Z, RB, L), BF16), vm((Z, RB, L), BF16), vm((Z - 1, RB, L), BF16), vm((Z - 1, RB, L), BF16),
-        vm((Z - 1, Y, RB, L), BF16), vm((Y, RB, L), BF16), vm((Y - 1, RB, L), BF16),
+        vm((Z, Y, RB, L), BF16), vm((NF, Y, RB, 2 * L), BF16), vm((NN + 1, Y, RB, L), BF16), vm((NN + 1, Y, RB, L), BF16),
+        vm((Y - 1, Z, RB, L), BF16), vm((Y - 1, NF, RB, 2 * L), BF16), vm((Y - 1, NN + 1, RB, L), BF16),
+        vm((Z, RB, L), BF16), vm((NF, RB, 2 * L), BF16), vm((NN + 1, RB, L), BF16),
+        vm((Z - 1, RB, L), BF16), vm((NF, RB, 2 * L), BF16), vm((NN, RB, L), BF16),
+        vm((NN, Y, RB, L), BF16), vm((Y, RB, L), BF16), vm((Y - 1, RB, L), BF16),
         stat, stats, stat, stats,
         halo, vm((Y, PAD, L), F32), halo, vm((Z, PAD, L), F32),
-        dma((3,)), dma((4,)), dma((4,)), dma((4,)), dma((4,)), dma((6,)), dma((6,)), dma((2,)), dma((2,)), dma((2,)), dma((2,)),
+        pltpu.SemaphoreType.REGULAR((6,)),
+        dma((5,)), dma((4,)), dma((4,)), dma((4,)), dma((4,)), dma((6,)), dma((6,)), dma((3,)), dma((3,)), dma((2,)), dma((2,)),
         dma((7,)), dma((7,)), dma((7,)), dma((7,)), dma((3, NC)), dma((NC,)), dma((3, NC)), dma((7, NC)),
-        *[dma((Y - 1,)) for _ in range(6)], *[dma((Z - 1,)) for _ in range(6)],
+        *[dma((Y - 1,)) for _ in range(8)], dma((Z - 1,)), dma((Z - 1,)), dma((NF,)), dma((NF,)), *[dma((NN,)) for _ in range(4)],
         dma((Y - 1,)), dma((Y - 1,)), dma((Z - 1,)), dma((Z - 1,)),
     ]
     shapes = (
@@ -591,21 +733,22 @@
         jax.ShapeDtypeStruct((K, L), F32),
         jax.ShapeDtypeStruct((1, L), F32),
     )
-    block_input, value_proj, gate_proj, out_proj, grad_output = (
+    norm_gain = norm_gain.reshape(1, L)
+    block_input, value_proj, gate_proj, conv_taps, norm_gain, out_proj, grad_output = (
         pltpu.with_memory_space_constraint(a, pltpu.HBM)
-        for a in (block_input, value_proj, gate_proj, out_proj, grad_output)
+        for a in (block_input, value_proj, gate_proj, conv_taps, norm_gain, out_proj, grad_output)
     )
     outs = pl.pallas_call(
         functools.partial(body, Z, Y, C, K),
         out_shape=shapes,
-        in_specs=[hbm, hbm, hbm, vmem, vmem, hbm, hbm],
+        in_specs=[hbm] * 7,
         out_specs=[vmem] * 6,
         scratch_shapes=scratch,
         compiler_params=pltpu.CompilerParams(
             collective_id=0, has_side_effects=True, vmem_limit_bytes=VMEM_LIMIT
         ),
         name="block_backward",
-    )(block_input, value_proj, gate_proj, conv_taps, norm_gain.reshape(1, L), out_proj, grad_output)
+    )(block_input, value_proj, gate_proj, conv_taps, norm_gain, out_proj, grad_output)
     outs = pl.pallas_call(
         write_out,
         out_shape=shapes,

time: 60.5 us -> 50.3 us (0.83)
  Pallas kernels: 58.3 us -> 49 us
  local copies, waits for them, and re-layouts: 1.37 us -> 0 us
    pallas_call x1, Pallas kernels: 57.5 us -> 48.1 us  [shards(): pl.pallas_call(functools.partial(body, Z, Y, C, K), out_shape=shapes, in_...]
    unnamed x4 -> x0, local copies, waits for them, and re-layouts: 1.37 us -> none
where the time goes in v3:
time: 50.3 us; the launch traced here: 49.6 us
  Pallas kernels  49 us (97%)
  between operations  0.64 us (1%)
    pallas_call x1, Pallas kernels, shards(): pl.pallas_call(functools.partial(body, Z, Y, C, K), out_shape=shapes, in_...  48.1 us

profile of v3, /device:TPU:2, one launch (start us, length us, event | category | flops | bytes accessed | tf_op | source)
XLA Modules:
  0.0 49.6 jit_solution(463414902862313842)
XLA Ops:
  0.6 48.1 %block_backward.1 = (bf16[1024,256]{1,0:T(8,128)(2,1)S(1)}, f32[64,128]{1,0:T(8,128)S(1)}, f32[64,128]{1,0:T(8,128)S(1)}, f32[64,128]{1,0:T(8,128)S(1)}, f32[31,128]{1,0:T(8,128)S(1)}, /*index=5*/f32[1,128]{1,0:T(1,128)S(1)}) custom-call(bf16[1024,2048]{1,0:T(8,128)(2,1)} %x_hbm.1, bf16[2048,128]{1,0:T(8,128)(2,1)} %vp_hbm.1, bf16[2048,128]{1,0:T(8,128)(2,1)} %gp_hbm.1, ...), custom_call_target="tpu_custom_call" | custom-call | tf_op jit(solution)/shard_map/block_backward/pallas_call | solution.py:741
  48.7 0.9 %write_out.1 = (bf16[1024,256]{1,0:T(8,128)(2,1)}, f32[64,128]{1,0:T(8,128)}, f32[64,128]{1,0:T(8,128)}, f32[64,128]{1,0:T(8,128)}, f32[31,128]{1,0:T(8,128)}, /*index=5*/f32[1,128]{1,0:T(1,128)}) custom-call(bf16[1024,256]{1,0:T(8,128)(2,1)S(1)} %get-tuple-element.18.refs_0_, f32[64,128]{1,0:T(8,128)S(1)} %get-tuple-element.19.refs_1_, ...), custom_call_target="tpu_custom_call" | custom-call | tf_op jit(solution)/shard_map/write_out/pallas_call | solution.py:752

commit v4 on v3

--- a/solution.py
+++ b/solution.py
@@ -20,8 +20,10 @@
 NP = 132
 HP = 164
 PAD = 32
-NN = 4
+NN = 2
 FAR0, NF = 3, 3
+NM = 2
+NO = NF + NM
 NC = 4
 
 
@@ -39,9 +41,9 @@
     ig, vg, gg, og, tg, ng,
     xv, gv, wvg, wo, wg, vbuf, sbuf, slope, hist, convp, nrm, nsl, inv, act, cs, vsf, gsf, sl, slg, acc,
     tail, halo_in, halo_out, halo_back, taps, gain,
-    actT, slT, wgo, wvf, wvn, wgn, yro, yrf, yrv, zso, zsf, zsv, zro, zrf, zrv, zrg, ysg, yrg, sta, star, stb, stbr, tgs, tgy, tgzs, tgz,
-    in_sem, l_sem, x_sem, g_sem, wo_ss, wo_rs, w_ss, w_rs, wy_ss, wy_rs, h_ss, h_rs, sa_ss, sa_rs, sb_ss, sb_rs, own_ss, fwd_ss, pf_ss, slg_rs,
-    yo_ss, yo_rs, yf_ss, yf_rs, yv_ss, yv_rs, yg_ss, yg_rs, zo_ss, zo_rs, zf_ss, zf_rs, zv_ss, zv_rs, zg_ss, zg_rs,
+    actT, slT, wof, won, wvf, wvm, wvn, yrof, yrf, yrv, zsof, zsf, zsv, zrof, zron, zrf, zrv, zrg, ysg, yrg, yson, yron, sta, star, stb, stbr, tgs, tgy, tgzs, tgz,
+    in_sem, l_sem, x_sem, g_sem, wo_ss, wo_rs, w_ss, w_rs, wy_ss, wy_rs, h_ss, h_rs, sa_ss, sa_rs, sb_ss, sb_rs, slg_ss, slg_rs,
+    yof_ss, yof_rs, yon_ss, yon_rs, yf_ss, yf_rs, yv_ss, yv_rs, yg_ss, yg_rs, zof_ss, zof_rs, zon_ss, zon_rs, zf_ss, zf_rs, zv_ss, zv_rs, zg_ss, zg_rs,
     ty_ss, ty_rs, tz_ss, tz_rs,
 ):
     z, y, x, c = (lax.axis_index(a) for a in ("z", "y", "x", "c"))
@@ -77,12 +79,19 @@
     nxt, prv = to(z=zn, y=yn), to(z=zb, y=yb)
     sent = []
 
+    def arrived(ref, rs):
+        pltpu.make_async_copy(ref, ref, rs).wait()
+
+    def sent_all(ref, ss):
+        sent.append((ref, ss))
+
+
     loads = [
         pltpu.make_async_copy(vp_hbm, wvg.at[:, pl.ds(0, L)], l_sem.at[0]),
-        pltpu.make_async_copy(gp_hbm, wvg.at[:, pl.ds(L, L)], l_sem.at[1]),
-        pltpu.make_async_copy(op_hbm, wo, l_sem.at[2]),
-        pltpu.make_async_copy(taps_hbm, taps, l_sem.at[3]),
-        pltpu.make_async_copy(gain_hbm, gain, l_sem.at[4]),
+        pltpu.make_async_copy(gp_hbm, wvg.at[:, pl.ds(L, L)], l_sem.at[0]),
+        pltpu.make_async_copy(op_hbm, wo, l_sem.at[1]),
+        pltpu.make_async_copy(taps_hbm, taps, l_sem.at[2]),
+        pltpu.make_async_copy(gain_hbm, gain, l_sem.at[3]),
     ]
     loads[0].start()
     loads[1].start()
@@ -141,8 +150,13 @@
                 pl.semaphore_wait(in_sem.at[2 * k + i], 1)
 
 
-    loads[0].wait()
-    loads[1].wait()
+    arrived(wvg, l_sem.at[0])
+
+    right, left = to(x=xp), to(x=xm)
+    partner = to(c=1 - c)
+
+    def piece(ref, q):
+        return ref.at[pl.ds(q * CH, CH)]
 
     def x_step(i, end):
         x_load(i).wait()
@@ -167,8 +181,6 @@
         x_step(i, False)
         return carry
 
-    x_step(0, False)
-
     pl.semaphore_wait(barrier, greeted)
     halo_m = remote(tail, halo_in, h_ss.at[0], h_rs.at[0], nxt)
 
@@ -178,37 +190,34 @@
 
     pass_on(0)
 
-    yq, zq = y % 2, z % 2
-    w_copies, w_own = [], []
-    for o in range(1, 8):
-        px, pc = xs[o // 2], cc[o % 2]
-        row = (px * 2 + pc) * DB
-        if o == 1:
-            for i in range(4):
-                at = pl.ds(pl.multiple_of(row + i * DQ, DQ), DQ)
-                w_own.append(remote(wvg.at[at], wg.at[0, i // 2, i % 2], wo_ss.at[i], wo_rs.at[i], tp_peers[0]))
-                w_own[-1].start()
-        else:
-            at = pl.ds(pl.multiple_of(row + (2 * yq + zq) * DQ, DQ), DQ)
-            w_copies.append(
-                remote(wvg.at[at], wg.at[o - 1, yq, zq], w_ss.at[o - 2], w_rs.at[o - 2], tp_peers[o - 1])
-            )
-            w_copies[-1].start()
-    sent.extend([*w_own, *w_copies])
-
-    lax.fori_loop(1, XC - 1, x_loop, 0)
+    yq = y % 2
+    y_pair = to(y=y + 1 - 2 * yq)
+
+    def w_start(part):
+        for o in range(2, 8):
+            row = (xs[o // 2] * 2 + cc[o % 2]) * DB + (2 * yq + part) * DQ
+            at = pl.ds(pl.multiple_of(row, DQ), DQ)
+            remote(
+                wvg.at[at], wg.at[o - 1, yq, part], w_ss.at[part], w_rs.at[part], tp_peers[o - 1]
+            ).start()
+        sent_all(wg.at[pl.ds(1, 6), yq, part], w_ss.at[part])
+
+    def w_on(part):
+        at = wg.at[pl.ds(1, 6), yq, part]
+        arrived(at, w_rs.at[part])
+        remote(at, at, wy_ss.at[part], wy_rs.at[part], y_pair).start()
+        sent_all(at, wy_ss.at[part])
+
+    w_start(0)
+    for i in range(4):
+        at = pl.ds(pl.multiple_of((xs[0] * 2 + cc[1]) * DB + i * DQ, DQ), DQ)
+        remote(wvg.at[at], wg.at[0, i // 2, i % 2], wo_ss.at[0], wo_rs.at[0], tp_peers[0]).start()
+    sent_all(wg.at[0], wo_ss.at[0])
+
+    lax.fori_loop(0, XC - 1, x_loop, 0)
 
     for cp in loads[2:]:
         cp.wait()
-
-    def g_loop(i, carry):
-        g_load(i).wait()
-        r = dot_nn(gv[pl.ds(pl.multiple_of(i * XR, XR), XR), :], wo[...])
-        for h in range(XR // T):
-            slope[pl.ds((i * (XR // T) + h) * NP, T), :] = r[h * T : (h + 1) * T]
-        return carry
-
-    lax.fori_loop(0, XC, g_loop, 0)
 
     lane = lax.broadcasted_iota(jnp.int32, (S, L), 1)
     zero = jnp.zeros((S, L), F32)
@@ -242,11 +251,10 @@
         return s1, s2
 
     def exchange(own, got, ss, rs):
-        copies = [remote(own, got.at[i], ss.at[i], rs.at[i], tp_peers[i]) for i in range(7)]
+        copies = [remote(own, got.at[i], ss.at[0], rs.at[0], tp_peers[i]) for i in range(7)]
         for cp in copies:
             cp.start()
-        sent.extend(copies)
-        return copies
+        sent_all(got, ss.at[0])
 
     def total(own, got, i):
         r = own[i]
@@ -269,23 +277,24 @@
     s1, s2 = lax.fori_loop(0, near_end, conv_block, (s1, s2))
     sta[0] = s1
     sta[1] = s2
-    ex = exchange(sta, star, sa_ss, sa_rs)
-
-    for cp in w_copies:
-        cp.wait_recv()
-    at = wg.at[pl.ds(1, 6), yq, zq]
-    w_on = [
-        remote(at, at, wy_ss.at[0], wy_rs.at[0], to(y=y + 1 - 2 * yq)),
-        remote(at, at, wy_ss.at[1], wy_rs.at[1], to(z=z + 1 - 2 * zq)),
-    ]
-    for cp in w_on:
-        cp.start()
-    sent.extend(w_on)
+    exchange(sta, star, sa_ss, sa_rs)
+    w_start(1)
+
+    def g_loop(i, carry):
+        g_load(i).wait()
+        r = dot_nn(gv[pl.ds(pl.multiple_of(i * XR, XR), XR), :], wo[...])
+        for h in range(XR // T):
+            slope[pl.ds((i * (XR // T) + h) * NP, T), :] = r[h * T : (h + 1) * T]
+        return carry
+
+    lax.fori_loop(0, XC, g_loop, 0)
+
     heard(0)
     pass_on(1)
 
-    for cp in ex:
-        cp.wait_recv()
+    w_on(0)
+
+    arrived(star, sa_rs.at[0])
     center = total(sta, star, 0)
     inverse = lax.rsqrt(total(sta, star, 1) - center * center + norm_floor)
     gains = gain[...]
@@ -313,9 +322,10 @@
     gsum, s1, s2 = lax.fori_loop(0, T // J, norm_block, (zero, zero, zero))
     stb[0] = s1
     stb[1] = s2
-    ex = exchange(stb, stbr, sb_ss, sb_rs)
+    exchange(stb, stbr, sb_ss, sb_rs)
     heard(1)
     pass_on(2)
+    w_on(1)
 
     def flip(src, dst, row0):
         def step(n, carry):
@@ -333,26 +343,35 @@
             put(yi, r[yi * RB : (yi + 1) * RB])
 
     def y_send(src, dst, ss, rs):
-        copies = []
         for d in range(1, Y):
-            copies.append(
-                remote(src.at[:, (y + d) % Y], dst.at[d - 1], ss.at[d - 1], rs.at[d - 1], y_peers[d - 1])
-            )
-            copies[-1].start()
-        sent.extend(copies)
-        return copies
-
-    def out_loop(zi, carry):
+            remote(src.at[:, (y + d) % Y], dst.at[d - 1], ss.at[0], rs.at[0], y_peers[d - 1]).start()
+        sent_all(dst, ss.at[0])
+
+    def near_of(e):
+        return (z + Z + 1 - 2 * e) % Z
+
+    def mid_of(e):
+        return (z + 2 + (Z - 4) * e) % Z
+
+    def out_put(dst, e):
         def put(yi, r):
-            wgo[zi, yi] = r
-
-        weight_block(actT, gv, zi, put)
-        return carry
-
-    lax.fori_loop(0, Z, out_loop, 0)
-
-    for cp in ex:
-        cp.wait_recv()
+            dst[e, yi] = r
+
+        return put
+
+    def out_near_loop(e, carry):
+        weight_block(actT, gv, near_of(e), out_put(won, e))
+        return carry
+
+    def out_far_loop(e, carry):
+        weight_block(actT, gv, (z + 2 + e) % Z, out_put(wof, e))
+        return carry
+
+    lax.fori_loop(0, NO, out_far_loop, 0)
+    weight_block(actT, gv, z, out_put(won, NN))
+    lax.fori_loop(0, NN, out_near_loop, 0)
+
+    arrived(stbr, sb_rs.at[0])
     slope_sum = total(stb, stbr, 0)
     cross_sum = total(stb, stbr, 1)
 
@@ -373,12 +392,7 @@
     def _():
         halo_c.start()
 
-    at = wg.at[pl.ds(1, 6), 1 - yq, zq]
-    remote(at, at, wy_ss.at[0], wy_rs.at[0], to(y=y + 1 - 2 * yq)).wait_recv()
-    w_z = remote(at, at, wy_ss.at[2], wy_rs.at[2], to(z=z + 1 - 2 * zq))
-    w_z.start()
-    sent.append(w_z)
-    yo = y_send(wgo, yro, yo_ss, yo_rs)
+    y_send(wof, yrof, yof_ss, yof_rs)
     for n in range(S - 1):
         cs[pl.ds(n * HP + T, PAD), :] = cs[pl.ds((n + 1) * HP, PAD), :]
     lax.fori_loop(PAD // J, T // J, cs_block, 0)
@@ -419,11 +433,9 @@
     for k in range(K):
         tgs[pl.ds(k, 1), :] = jnp.sum(sums[k], axis=0, keepdims=True)
     tgs[pl.ds(K, 1), :] = jnp.sum(gsum, axis=0, keepdims=True)
-    ty = []
     for d in range(1, Y):
-        ty.append(remote(tgs, tgy.at[y], ty_ss.at[d - 1], ty_rs.at[d - 1], y_peers[d - 1]))
-        ty[-1].start()
-    sent.extend(ty)
+        remote(tgs, tgy.at[y], ty_ss.at[0], ty_rs.at[0], y_peers[d - 1]).start()
+    sent_all(tgy.at[pl.ds(0, Y - 1)], ty_ss.at[0])
     tgy[y] = tgs[...]
 
 
@@ -446,27 +458,34 @@
 
     lax.fori_loop(0, S, to_bf16, 0)
 
-    def piece(ref, q):
-        return ref.at[pl.ds(q * CH, CH)]
-
-    def own_copy(way, slot, q, dev):
-        return remote(piece(sl, q), piece(slg.at[slot], q), own_ss.at[way, q], slg_rs.at[slot, q], dev)
-
-    right, left = to(x=xp), to(x=xm)
-    partner = to(c=1 - c)
-    up = [own_copy(0, 1, q, right) for q in range(NC)]
-    down = [own_copy(1, 2, q, left) for q in range(NC)]
-    over = [own_copy(2, 0, q, partner) for q in range(NC)]
+    RS = (0, 1, 5, 9, 13, 14, 15)
+
+    def pass_slope(src, slot, q, sem, dev):
+        return remote(piece(src, q), piece(slg.at[slot], q), slg_ss.at[0], sem, dev)
+
+    def own_copy(slot, q, dev):
+        return pass_slope(sl, slot, q, slg_rs.at[RS[slot] + (q if slot else 0)], dev)
+
+    up = [own_copy(1, q, right) for q in range(NC)]
+    down = [own_copy(2, q, left) for q in range(NC)]
+    over = [own_copy(0, q, partner) for q in range(NC)]
     half = NC // 2
     for i in range(NC):
         up[i].start()
-        down[(i + half) % NC].start()
+        down[NC - 1 - i].start()
     for i in range(NC):
         over[i].start()
-    sent.extend([*up, *down, *over])
-
-    flip(vsf, slT, 0)
-    flip(gsf, slT, L)
+    sent_all(slg, slg_ss.at[0])
+
+    heard(2)
+    for e in range(NN):
+        remote(won.at[e], zron.at[e], zon_ss.at[0], zon_rs.at[0], to(z=near_of(e))).start()
+    sent_all(zron, zon_ss.at[0])
+
+    diagonal = (
+        lax.broadcasted_iota(jnp.int32, (2 * L, 2 * L), 0) == lax.broadcasted_iota(jnp.int32, (2 * L, 2 * L), 1)
+    ).astype(F32).astype(BF16)
+    slT[...] = dot_nt(diagonal, sl[...]).astype(BF16)
 
     def far_loop(e, carry):
         def put(yi, r):
@@ -475,39 +494,25 @@
         weight_block(slT, xv, (z + FAR0 + e) % Z, put)
         return carry
 
-    def near_of(e):
-        return (z + Z + (1 + e // 2) * (1 - 2 * (e % 2))) % Z
-
-    def near_from(e):
-        return (z + Z - (1 + e // 2) * (1 - 2 * (e % 2))) % Z
-
-    def gate_send(e):
-        return remote(wgn.at[e], zrg.at[e], zg_ss.at[e], zg_rs.at[e], to(z=near_of(e)))
-
-    def near_put(e):
-        def put(yi, r):
-            wvn[e, yi] = r[:, :L]
-            wgn[e, yi] = r[:, L:]
-
-        return put
+    def mid_loop(e, carry):
+        weight_block(slT, xv, mid_of(e), out_put(wvm, e))
+        return carry
+
+    def near_send(e):
+        return remote(wvn.at[e], zrg.at[e], zg_ss.at[0], zg_rs.at[0], to(z=near_of(e)))
 
     def near_loop(e, carry):
-        weight_block(slT, xv, near_of(e), near_put(e))
-        gate_send(e).start()
-        return carry
-
-    heard(2)
+        weight_block(slT, xv, near_of(e), out_put(wvn, e))
+        near_send(e).start()
+        return carry
+
     lax.fori_loop(0, NF, far_loop, 0)
-    yf = y_send(wvf, yrf, yf_ss, yf_rs)
+    y_send(wvf, yrf, yf_ss, yf_rs)
     lax.fori_loop(0, NN, near_loop, 0)
-    weight_block(slT, xv, z, near_put(NN))
-    yv = y_send(wvn, yrv, yv_ss, yv_rs)
-    zg = [gate_send(e) for e in range(NN)]
-    sent.extend(zg)
-
-    for cp in yo:
-        cp.wait_recv()
-    zo = second(Z, Y, y, z, wgo, yro, zso, zro, zo_ss, zo_rs, z_peers, remote, sent)
+    sent_all(zrg, zg_ss.at[0])
+    lax.fori_loop(0, NM, mid_loop, 0)
+    y_send(wvm, yrv, yv_ss, yv_rs)
+    weight_block(slT, xv, z, out_put(wvn, NN))
 
     def weights_from(slot):
         core = 1 if slot == 0 or slot > 3 else 0
@@ -527,99 +532,91 @@
         acc[at, :] += dot_nt(slg[slot, at, :], weights_from(slot))
 
     def pf(slot, q):
-        cp = remote(
-            piece(slg.at[slot], q), piece(slg.at[slot + 3], q), pf_ss.at[slot - 1, q], slg_rs.at[slot + 3, q], partner
-        )
+        sem = slg_rs.at[RS[slot + 3] + (q if slot == 3 else 0)]
+        cp = pass_slope(slg.at[slot], slot + 3, q, sem, partner)
         cp.start()
-        sent.append(cp)
         return cp
+
+    def near_sum(own, got, z_rs, ys, yr, y_ss, y_rs):
+        arrived(got, z_rs.at[0])
+        for yi in range(Y):
+            r = own[NN, yi].astype(F32)
+            for e in range(NN):
+                r = r + got[e, yi].astype(F32)
+            ys[yi] = r.astype(BF16)
+        for d in range(1, Y):
+            remote(ys.at[(y + d) % Y], yr.at[d - 1], y_ss.at[0], y_rs.at[0], y_peers[d - 1]).start()
+        sent_all(yr, y_ss.at[0])
 
     fwd = {}
     pfs = {}
-    for i in range(NC):
-        q = i
-        up[q].wait_recv()
-        if i < half:
-            fwd[q] = remote(piece(slg.at[1], q), piece(slg.at[3], q), fwd_ss.at[q], slg_rs.at[3, q], right)
-            fwd[q].start()
-        pfs[1, q] = pf(1, q)
-        q2 = (i + half) % NC
-        down[q2].wait_recv()
-        if i < half:
-            fwd[q2] = remote(piece(slg.at[2], q2), piece(slg.at[3], q2), fwd_ss.at[q2], slg_rs.at[3, q2], left)
-            fwd[q2].start()
-        pfs[2, q2] = pf(2, q2)
-        over[i].wait_recv()
-        if i == 1:
-            for cp in w_own:
-                cp.wait_recv()
-            for k, yi in ((1, yq), (2, 1 - yq)):
-                at = wg.at[pl.ds(1, 6), yi, 1 - zq]
-                remote(at, at, wy_ss.at[k], wy_rs.at[k], to(z=z + 1 - 2 * zq)).wait_recv()
-        for j in {0: (), 1: (0, 1)}.get(i, (i,)):
-            add(0, j)
-            add(1, j)
-            add(2, (j + half) % NC)
-        if i == 1:
-            for cp in ty:
-                cp.wait_recv()
-            t = tgy[0]
-            for yi in range(1, Y):
-                t = t + tgy[yi]
-            tgzs[...] = t
-            tgz[z] = t
-            tz = []
-            for d in range(1, Z):
-                tz.append(remote(tgzs, tgz.at[z], tz_ss.at[d - 1], tz_rs.at[d - 1], z_peers[d - 1]))
-                tz[-1].start()
-            sent.extend(tz)
-        if i == 2:
-            for cp in yf:
-                cp.wait_recv()
-            zf = []
-            for e in range(NF):
-                r = wvf[e, y].astype(F32)
-                for d in range(Y - 1):
-                    r = r + yrf[d, e].astype(F32)
-                zsf[e] = r.astype(BF16)
-                zf.append(remote(zsf.at[e], zrf.at[e], zf_ss.at[e], zf_rs.at[e], to(z=(z + FAR0 + e) % Z)))
-                zf[-1].start()
-            sent.extend(zf)
-            for cp in zg:
-                cp.wait_recv()
-            for yi in range(Y):
-                r = wgn[NN, yi].astype(F32)
-                for e in range(NN):
-                    r = r + zrg[e, yi].astype(F32)
-                ysg[yi] = r.astype(BF16)
-            yg = []
-            for d in range(1, Y):
-                yg.append(
-                    remote(ysg.at[(y + d) % Y], yrg.at[d - 1], yg_ss.at[d - 1], yg_rs.at[d - 1], y_peers[d - 1])
-                )
-                yg[-1].start()
-            sent.extend(yg)
-        if i == 3:
-            for cp in yv:
-                cp.wait_recv()
-            zv = []
-            for e in range(NN + 1):
-                r = wvn[e, y].astype(F32)
-                for d in range(Y - 1):
-                    r = r + yrv[d, e].astype(F32)
-                zsv[e] = r.astype(BF16)
-                if e < NN:
-                    zv.append(remote(zsv.at[e], zrv.at[e], zv_ss.at[e], zv_rs.at[e], to(z=near_of(e))))
-                    zv[-1].start()
-            sent.extend(zv)
-    sent.extend(fwd.values())
-    for q in range(NC):
-        pfs[1, q].wait_recv()
-        add(4, q)
-        pfs[2, q].wait_recv()
-        add(5, q)
-
-    order = [q for i in range(half) for q in (i, i + half)]
+
+    def take(i):
+        for slot, q, copies, way in ((1, i, up, right), (2, NC - 1 - i, down, left)):
+            copies[q].wait_recv()
+            if i < half:
+                fwd[q] = pass_slope(slg.at[slot], 3, q, slg_rs.at[RS[3] + q], way)
+                fwd[q].start()
+            pfs[slot, q] = pf(slot, q)
+
+    def use(i):
+        add(0, i)
+        add(1, i)
+        add(2, NC - 1 - i)
+
+    take(0)
+    arrived(tgy.at[pl.ds(0, Y - 1)], ty_rs.at[0])
+    t = tgy[0]
+    for yi in range(1, Y):
+        t = t + tgy[yi]
+    tgzs[...] = t.astype(BF16)
+    tgz[z] = t.astype(BF16)
+    for d in range(1, Z):
+        remote(tgzs, tgz.at[z], tz_ss.at[0], tz_rs.at[0], z_peers[d - 1]).start()
+    sent_all(tgz.at[pl.ds(0, Z - 1)], tz_ss.at[0])
+    arrived(yrof, yof_rs.at[0])
+    for e in range(NO):
+        r = wof[e, y].astype(F32)
+        for d in range(Y - 1):
+            r = r + yrof[d, e].astype(F32)
+        zsof[e] = r.astype(BF16)
+        remote(zsof.at[e], zrof.at[e], zof_ss.at[0], zof_rs.at[0], to(z=(z + 2 + e) % Z)).start()
+    sent_all(zrof, zof_ss.at[0])
+    near_sum(won, zron, zon_rs, yson, yron, yon_ss, yon_rs)
+    take(1)
+    arrived(yrf, yf_rs.at[0])
+    for e in range(NF):
+        r = wvf[e, y].astype(F32)
+        for d in range(Y - 1):
+            r = r + yrf[d, e].astype(F32)
+        zsf[e] = r.astype(BF16)
+        remote(zsf.at[e], zrf.at[e], zf_ss.at[0], zf_rs.at[0], to(z=(z + FAR0 + e) % Z)).start()
+    sent_all(zrf, zf_ss.at[0])
+    arrived(slg.at[0], slg_rs.at[RS[0]])
+    arrived(wg.at[0], wo_rs.at[0])
+    for part in range(2):
+        arrived(wg.at[pl.ds(1, 6), 1 - yq, part], wy_rs.at[part])
+    use(0)
+    take(2)
+    arrived(yrv, yv_rs.at[0])
+    for e in range(NM):
+        r = wvm[e, y].astype(F32)
+        for d in range(Y - 1):
+            r = r + yrv[d, e].astype(F32)
+        zsv[e] = r.astype(BF16)
+        remote(zsv.at[e], zrv.at[e], zv_ss.at[0], zv_rs.at[0], to(z=mid_of(e))).start()
+    sent_all(zrv, zv_ss.at[0])
+    take(3)
+    use(1)
+    use(2)
+    use(3)
+    near_sum(wvn, zrg, zg_rs, ysg, yrg, yg_ss, yg_rs)
+    for slot in (4, 5):
+        arrived(slg.at[slot], slg_rs.at[RS[slot]])
+        for q in range(NC):
+            add(slot, q)
+
+    order = [q for i in range(half) for q in (i, NC - 1 - i)]
     for q in order:
         fwd[q].wait_recv()
         pfs[3, q] = pf(3, q)
@@ -629,38 +626,32 @@
         add(6, q)
     ig[...] = acc[...].astype(BF16)
 
-    def finish(copies, own, got, count):
-        for cp in copies:
-            cp.wait_recv()
-        r = own.astype(F32)
-        for d in range(count - 1):
-            r = r + got[d].astype(F32)
-        return r
-
-    og[...] = finish(zo, zso[z], zro, Z)
-    for cp in tz:
-        cp.wait_recv()
-    t = tgz[0]
+    arrived(zrof, zof_rs.at[0])
+    arrived(yron, yon_rs.at[0])
+    r = yson[y].astype(F32)
+    for d in range(Y - 1):
+        r = r + yron[d].astype(F32)
+    for e in range(NO):
+        r = r + zrof[e].astype(F32)
+    og[...] = r
+    arrived(tgz.at[pl.ds(0, Z - 1)], tz_rs.at[0])
+    t = tgz[0].astype(F32)
     for zi in range(1, Z):
-        t = t + tgz[zi]
+        t = t + tgz[zi].astype(F32)
     tg[...] = t[:K]
     ng[...] = t[K : K + 1]
-    for cp in [*zf, *zv, *yg]:
-        cp.wait_recv()
-    far = zrf[0].astype(F32)
-    for e in range(1, NF):
-        far = far + zrf[e].astype(F32)
-    r = far[:, :L] + zsv[NN].astype(F32)
-    for e in range(NN):
-        r = r + zrv[e].astype(F32)
-    vg[...] = r
-    r = far[:, L:] + ysg[y].astype(F32)
-    for d in range(Y - 1):
-        r = r + yrg[d].astype(F32)
-    gg[...] = r
-
-    for cp in sent:
-        cp.wait_send()
+    arrived(zrf, zf_rs.at[0])
+    arrived(zrv, zv_rs.at[0])
+    arrived(yrg, yg_rs.at[0])
+    r = ysg[y].astype(F32)
+    for got, count in ((yrg, Y - 1), (zrf, NF), (zrv, NM)):
+        for e in range(count):
+            r = r + got[e].astype(F32)
+    vg[...] = r[:, :L]
+    gg[...] = r[:, L:]
+
+    for ref, ss in sent:
+        arrived(ref, ss)
 
     @pl.when(jnp.logical_not(last))
     def _():
@@ -669,23 +660,6 @@
     @pl.when(jnp.logical_not(first))
     def _():
         halo_c.wait_send()
-
-
-def second(Z, Y, y, z, own, got, zs, zr, ss, rs, z_peers, remote, sent):
-    def step(zi, carry):
-        r = own[zi, y].astype(F32)
-        for d in range(Y - 1):
-            r = r + got[d, zi].astype(F32)
-        zs[zi] = r.astype(BF16)
-        return carry
-
-    lax.fori_loop(0, Z, step, 0)
-    copies = []
-    for d in range(1, Z):
-        copies.append(remote(zs.at[(z + d) % Z], zr.at[d - 1], ss.at[d - 1], rs.at[d - 1], z_peers[d - 1]))
-        copies[-1].start()
-    sent.extend(copies)
-    return copies
 
 
 def write_out(*refs):
@@ -712,18 +686,18 @@
         near, near, vm((rows, 2 * L), BF16), vm((7, rows, 2 * L), BF16), vm((rows, DB), F32),
         halo, halo, halo, halo, vm((K, L), F32), vm((1, L), F32),
         vm((L, rows), BF16), vm((2 * L, rows), BF16),
-        vm((Z, Y, RB, L), BF16), vm((NF, Y, RB, 2 * L), BF16), vm((NN + 1, Y, RB, L), BF16), vm((NN + 1, Y, RB, L), BF16),
-        vm((Y - 1, Z, RB, L), BF16), vm((Y - 1, NF, RB, 2 * L), BF16), vm((Y - 1, NN + 1, RB, L), BF16),
-        vm((Z, RB, L), BF16), vm((NF, RB, 2 * L), BF16), vm((NN + 1, RB, L), BF16),
-        vm((Z - 1, RB, L), BF16), vm((NF, RB, 2 * L), BF16), vm((NN, RB, L), BF16),
-        vm((NN, Y, RB, L), BF16), vm((Y, RB, L), BF16), vm((Y - 1, RB, L), BF16),
+        vm((NO, Y, RB, L), BF16), vm((NN + 1, Y, RB, L), BF16),
+        vm((NF, Y, RB, 2 * L), BF16), vm((NM, Y, RB, 2 * L), BF16), vm((NN + 1, Y, RB, 2 * L), BF16),
+        vm((Y - 1, NO, RB, L), BF16), vm((Y - 1, NF, RB, 2 * L), BF16), vm((Y - 1, NM, RB, 2 * L), BF16),
+        vm((NO, RB, L), BF16), vm((NF, RB, 2 * L), BF16), vm((NM, RB, 2 * L), BF16),
+        vm((NO, RB, L), BF16), vm((NN, Y, RB, L), BF16), vm((NF, RB, 2 * L), BF16), vm((NM, RB, 2 * L), BF16),
+        vm((NN, Y, RB, 2 * L), BF16), vm((Y, RB, 2 * L), BF16), vm((Y - 1, RB, 2 * L), BF16),
+        vm((Y, RB, L), BF16), vm((Y - 1, RB, L), BF16),
         stat, stats, stat, stats,
-        halo, vm((Y, PAD, L), F32), halo, vm((Z, PAD, L), F32),
+        halo, vm((Y, PAD, L), F32), vm((PAD, L), BF16), vm((Z, PAD, L), BF16),
         pltpu.SemaphoreType.REGULAR((6,)),
-        dma((5,)), dma((4,)), dma((4,)), dma((4,)), dma((4,)), dma((6,)), dma((6,)), dma((3,)), dma((3,)), dma((2,)), dma((2,)),
-        dma((7,)), dma((7,)), dma((7,)), dma((7,)), dma((3, NC)), dma((NC,)), dma((3, NC)), dma((7, NC)),
-        *[dma((Y - 1,)) for _ in range(8)], dma((Z - 1,)), dma((Z - 1,)), dma((NF,)), dma((NF,)), *[dma((NN,)) for _ in range(4)],
-        dma((Y - 1,)), dma((Y - 1,)), dma((Z - 1,)), dma((Z - 1,)),
+        dma((4,)), dma((4,)), dma((4,)), *[dma((1,)) for _ in range(2)], *[dma((2,)) for _ in range(6)],
+        *[dma((1,)) for _ in range(4)], dma((1,)), dma((19,)), *[dma((1,)) for _ in range(24)],
     ]
     shapes = (
         jax.ShapeDtypeStruct((rows, DB), BF16),

time: 50.3 us -> 46.1 us (0.917)
  the two profiles are of different devices: /device:TPU:2 before, /device:TPU:121 now
where the time goes in v4:
time: 46.1 us; the launch traced here: 46 us
  Pallas kernels  45.4 us (98%)
  between operations  0.64 us (1%)
    pallas_call x1, Pallas kernels, shards(): pl.pallas_call(functools.partial(body, Z, Y, C, K), out_shape=shapes, in_...  44.5 us

profile of v4, /device:TPU:121, one launch (start us, length us, event | category | flops | bytes accessed | tf_op | source)
XLA Modules:
  0.0 46.0 jit_solution(3460993567291771166)
XLA Ops:
  0.6 44.5 %block_backward.1 = (bf16[1024,256]{1,0:T(8,128)(2,1)S(1)}, f32[64,128]{1,0:T(8,128)S(1)}, f32[64,128]{1,0:T(8,128)S(1)}, f32[64,128]{1,0:T(8,128)S(1)}, f32[31,128]{1,0:T(8,128)S(1)}, /*index=5*/f32[1,128]{1,0:T(1,128)S(1)}) custom-call(bf16[1024,2048]{1,0:T(8,128)(2,1)} %x_hbm.1, bf16[2048,128]{1,0:T(8,128)(2,1)} %vp_hbm.1, bf16[2048,128]{1,0:T(8,128)(2,1)} %gp_hbm.1, ...), custom_call_target="tpu_custom_call" | custom-call | tf_op jit(solution)/shard_map/block_backward/pallas_call | solution.py:715
  45.2 0.9 %write_out.1 = (bf16[1024,256]{1,0:T(8,128)(2,1)}, f32[64,128]{1,0:T(8,128)}, f32[64,128]{1,0:T(8,128)}, f32[64,128]{1,0:T(8,128)}, f32[31,128]{1,0:T(8,128)}, /*index=5*/f32[1,128]{1,0:T(1,128)}) custom-call(bf16[1024,256]{1,0:T(8,128)(2,1)S(1)} %get-tuple-element.18.refs_0_, f32[64,128]{1,0:T(8,128)S(1)} %get-tuple-element.19.refs_1_, ...), custom_call_target="tpu_custom_call" | custom-call | tf_op jit(solution)/shard_map/write_out/pallas_call | solution.py:726

commit v5 on v4

--- a/solution.py
+++ b/solution.py
@@ -25,6 +25,7 @@
 NM = 2
 NO = NF + NM
 NC = 4
+EARLY = (0, 3)
 
 
 def dot_nn(a, b):
@@ -40,9 +41,9 @@
     x_hbm, vp_hbm, gp_hbm, taps_hbm, gain_hbm, op_hbm, g_hbm,
     ig, vg, gg, og, tg, ng,
     xv, gv, wvg, wo, wg, vbuf, sbuf, slope, hist, convp, nrm, nsl, inv, act, cs, vsf, gsf, sl, slg, acc,
-    tail, halo_in, halo_out, halo_back, taps, gain,
+    sqb, er, msf, msl, mr, tail, halo_in, halo_out, halo_back, taps, gain,
     actT, slT, wof, won, wvf, wvm, wvn, yrof, yrf, yrv, zsof, zsf, zsv, zrof, zron, zrf, zrv, zrg, ysg, yrg, yson, yron, sta, star, stb, stbr, tgs, tgy, tgzs, tgz,
-    in_sem, l_sem, x_sem, g_sem, wo_ss, wo_rs, w_ss, w_rs, wy_ss, wy_rs, h_ss, h_rs, sa_ss, sa_rs, sb_ss, sb_rs, slg_ss, slg_rs,
+    in_sem, l_sem, x_sem, g_sem, wo_ss, wo_rs, w_ss, w_rs, wy_ss, wy_rs, h_ss, h_rs, sa_ss, sa_rs, sb_ss, sb_rs, slg_ss, slg_rs, mr_rs, er_ss, er_rs,
     yof_ss, yof_rs, yon_ss, yon_rs, yf_ss, yf_rs, yv_ss, yv_rs, yg_ss, yg_rs, zof_ss, zof_rs, zon_ss, zon_rs, zf_ss, zf_rs, zv_ss, zv_rs, zg_ss, zg_rs,
     ty_ss, ty_rs, tz_ss, tz_rs,
 ):
@@ -158,6 +159,22 @@
     def piece(ref, q):
         return ref.at[pl.ds(q * CH, CH)]
 
+    def early_own(k):
+        src = piece(sqb, EARLY[k])
+        return [
+            remote(src, er.at[0, k], er_ss.at[0], er_rs.at[k], right),
+            remote(src, er.at[1, k], er_ss.at[0], er_rs.at[2 + k], left),
+        ]
+
+    def early_on(k):
+        return remote(er.at[k, k], er.at[2, k], er_ss.at[0], er_rs.at[4 + k], (right, left)[k])
+
+    def early_over(i, k):
+        return remote(er.at[i, k], er.at[i + 3, k], er_ss.at[0], er_rs.at[6 + 2 * i + k], partner)
+
+    def early_arrived(i, k):
+        arrived(er.at[i, k], er_rs.at[2 * i + k])
+
     def x_step(i, end):
         x_load(i).wait()
         res = dot_nn(xv[pl.ds(pl.multiple_of(i * XR, XR), XR), :], wvg[...])
@@ -169,6 +186,9 @@
             part = slice(h * T, (h + 1) * T)
             vbuf[pl.ds(n * NP, T), :] = v[part]
             sbuf[pl.ds(n * NP, T), :] = s[part]
+            at = pl.ds(pl.multiple_of(n * T, T), T)
+            sqb[at, pl.ds(0, L)] = s[part].astype(BF16)
+            sqb[at, pl.ds(L, L)] = (v[part] * s[part] * (1.0 - s[part])).astype(BF16)
             hist[pl.ds(n * HP + PAD, T), :] = m[part]
             if end and h == XR // T - 1:
                 tail[...] = m[XR - PAD :]
@@ -279,6 +299,8 @@
     sta[1] = s2
     exchange(sta, star, sa_ss, sa_rs)
     w_start(1)
+    for cp in early_own(1):
+        cp.start()
 
     def g_loop(i, carry):
         g_load(i).wait()
@@ -325,6 +347,8 @@
     exchange(stb, stbr, sb_ss, sb_rs)
     heard(1)
     pass_on(2)
+    for cp in early_own(0):
+        cp.start()
     w_on(1)
 
     def flip(src, dst, row0):
@@ -370,6 +394,11 @@
     lax.fori_loop(0, NO, out_far_loop, 0)
     weight_block(actT, gv, z, out_put(won, NN))
     lax.fori_loop(0, NN, out_near_loop, 0)
+
+    for i in range(2):
+        early_arrived(i, 1)
+        early_over(i, 1).start()
+    early_on(1).start()
 
     arrived(stbr, sb_rs.at[0])
     slope_sum = total(stb, stbr, 0)
@@ -409,6 +438,7 @@
         for j in range(J):
             t = t0 + j
             s = near(sbuf, t)
+            msf[pl.ds(t, S, stride=NP), :] = r[j]
             rs = r[j] * s
             vsf[pl.ds(t, S, stride=NP), :] = rs
             gsf[pl.ds(t, S, stride=NP), :] = rs * near(vbuf, t) * (1.0 - s)
@@ -429,6 +459,12 @@
                     sums[k] = sums[k] + e[j] * m
         return tuple(sums)
 
+    for i in range(2):
+        early_arrived(i, 0)
+        early_over(i, 0).start()
+    early_on(0).start()
+    sent_all(er, er_ss.at[0])
+
     sums = lax.fori_loop(0, T // 8, tap_block, tuple(zero for _ in range(K)))
     for k in range(K):
         tgs[pl.ds(k, 1), :] = jnp.sum(sums[k], axis=0, keepdims=True)
@@ -452,6 +488,7 @@
 
     def to_bf16(n, carry):
         at = pl.ds(pl.multiple_of(n * T, T), T)
+        msl[at, :] = msf[pl.ds(n * NP, T), :].astype(BF16)
         sl[at, pl.ds(0, L)] = vsf[pl.ds(n * NP, T), :].astype(BF16)
         sl[at, pl.ds(L, L)] = gsf[pl.ds(n * NP, T), :].astype(BF16)
         return carry
@@ -460,38 +497,48 @@
 
     RS = (0, 1, 5, 9, 13, 14, 15)
 
+    def held(slot, q):
+        return mr.at[slot - 1, EARLY.index(q)] if q in EARLY else piece(slg.at[slot], q)
+
     def pass_slope(src, slot, q, sem, dev):
-        return remote(piece(src, q), piece(slg.at[slot], q), slg_ss.at[0], sem, dev)
+        return remote(src, held(slot, q), slg_ss.at[1 if q in EARLY else 0], sem, dev)
 
     def own_copy(slot, q, dev):
-        return pass_slope(sl, slot, q, slg_rs.at[RS[slot] + (q if slot else 0)], dev)
+        return pass_slope(piece(msl if q in EARLY else sl, q), slot, q, slg_rs.at[RS[slot] + q], dev)
 
     up = [own_copy(1, q, right) for q in range(NC)]
     down = [own_copy(2, q, left) for q in range(NC)]
-    over = [own_copy(0, q, partner) for q in range(NC)]
+    over = [remote(piece(sl, q), piece(slg.at[0], q), slg_ss.at[0], slg_rs.at[0], partner) for q in range(NC)]
     half = NC // 2
     for i in range(NC):
         up[i].start()
         down[NC - 1 - i].start()
     for i in range(NC):
         over[i].start()
-    sent_all(slg, slg_ss.at[0])
+    sent_all(slg.at[pl.ds(0, 4)], slg_ss.at[0])
+    sent_all(mr, slg_ss.at[1])
 
     heard(2)
     for e in range(NN):
         remote(won.at[e], zron.at[e], zon_ss.at[0], zon_rs.at[0], to(z=near_of(e))).start()
     sent_all(zron, zon_ss.at[0])
-
     diagonal = (
         lax.broadcasted_iota(jnp.int32, (2 * L, 2 * L), 0) == lax.broadcasted_iota(jnp.int32, (2 * L, 2 * L), 1)
     ).astype(F32).astype(BF16)
     slT[...] = dot_nt(diagonal, sl[...]).astype(BF16)
 
+    def far_of(e):
+        return (z + FAR0 + 1 - e % 2 + e // 2) % Z
+
     def far_loop(e, carry):
         def put(yi, r):
             wvf[e, yi] = r
 
-        weight_block(slT, xv, (z + FAR0 + e) % Z, put)
+        weight_block(slT, xv, far_of(e), put)
+        for d in range(1, Y):
+            remote(
+                wvf.at[e, (y + d) % Y], yrf.at[d - 1, e], yf_ss.at[0], yf_rs.at[e], y_peers[d - 1]
+            ).start()
         return carry
 
     def mid_loop(e, carry):
@@ -507,7 +554,7 @@
         return carry
 
     lax.fori_loop(0, NF, far_loop, 0)
-    y_send(wvf, yrf, yf_ss, yf_rs)
+    sent_all(yrf, yf_ss.at[0])
     lax.fori_loop(0, NN, near_loop, 0)
     sent_all(zrg, zg_ss.at[0])
     lax.fori_loop(0, NM, mid_loop, 0)
@@ -529,11 +576,21 @@
 
     def add(slot, q):
         at = pl.ds(q * CH, CH)
-        acc[at, :] += dot_nt(slg[slot, at, :], weights_from(slot))
+        if slot and q in EARLY:
+            k = EARLY.index(q)
+            m = mr[slot - 1, k].astype(F32)
+            f = er[slot - 1, k].astype(F32)
+            block = jnp.concatenate([m * f[:, :L], m * f[:, L:]], axis=1).astype(BF16)
+        else:
+            block = slg[slot, at, :]
+        acc[at, :] += dot_nt(block, weights_from(slot))
 
     def pf(slot, q):
-        sem = slg_rs.at[RS[slot + 3] + (q if slot == 3 else 0)]
-        cp = pass_slope(slg.at[slot], slot + 3, q, sem, partner)
+        if slot == 3:
+            sem = slg_rs.at[RS[6] + q]
+        else:
+            sem = mr_rs.at[slot - 1] if q in EARLY else slg_rs.at[RS[slot + 3]]
+        cp = pass_slope(held(slot, q), slot + 3, q, sem, partner)
         cp.start()
         return cp
 
@@ -555,7 +612,7 @@
         for slot, q, copies, way in ((1, i, up, right), (2, NC - 1 - i, down, left)):
             copies[q].wait_recv()
             if i < half:
-                fwd[q] = pass_slope(slg.at[slot], 3, q, slg_rs.at[RS[3] + q], way)
+                fwd[q] = pass_slope(held(slot, q), 3, q, slg_rs.at[RS[3] + q], way)
                 fwd[q].start()
             pfs[slot, q] = pf(slot, q)
 
@@ -565,6 +622,8 @@
         add(2, NC - 1 - i)
 
     take(0)
+    early_arrived(2, 1)
+    early_over(2, 1).start()
     arrived(tgy.at[pl.ds(0, Y - 1)], ty_rs.at[0])
     t = tgy[0]
     for yi in range(1, Y):
@@ -582,15 +641,16 @@
         zsof[e] = r.astype(BF16)
         remote(zsof.at[e], zrof.at[e], zof_ss.at[0], zof_rs.at[0], to(z=(z + 2 + e) % Z)).start()
     sent_all(zrof, zof_ss.at[0])
-    near_sum(won, zron, zon_rs, yson, yron, yon_ss, yon_rs)
     take(1)
-    arrived(yrf, yf_rs.at[0])
+    early_arrived(2, 0)
+    early_over(2, 0).start()
     for e in range(NF):
+        arrived(yrf.at[:, e], yf_rs.at[e])
         r = wvf[e, y].astype(F32)
         for d in range(Y - 1):
             r = r + yrf[d, e].astype(F32)
         zsf[e] = r.astype(BF16)
-        remote(zsf.at[e], zrf.at[e], zf_ss.at[0], zf_rs.at[0], to(z=(z + FAR0 + e) % Z)).start()
+        remote(zsf.at[e], zrf.at[e], zf_ss.at[0], zf_rs.at[0], to(z=far_of(e))).start()
     sent_all(zrf, zf_ss.at[0])
     arrived(slg.at[0], slg_rs.at[RS[0]])
     arrived(wg.at[0], wo_rs.at[0])
@@ -606,17 +666,23 @@
         zsv[e] = r.astype(BF16)
         remote(zsv.at[e], zrv.at[e], zv_ss.at[0], zv_rs.at[0], to(z=mid_of(e))).start()
     sent_all(zrv, zv_ss.at[0])
+    near_sum(won, zron, zon_rs, yson, yron, yon_ss, yon_rs)
     take(3)
     use(1)
     use(2)
     use(3)
     near_sum(wvn, zrg, zg_rs, ysg, yrg, yg_ss, yg_rs)
     for slot in (4, 5):
-        arrived(slg.at[slot], slg_rs.at[RS[slot]])
+        arrived(slg.at[slot, pl.ds(CH, 2 * CH)], slg_rs.at[RS[slot]])
+        arrived(mr.at[slot - 1], mr_rs.at[slot - 4])
+        for k in range(2):
+            early_arrived(slot - 1, k)
         for q in range(NC):
             add(slot, q)
 
     order = [q for i in range(half) for q in (i, NC - 1 - i)]
+    for k in range(2):
+        early_arrived(5, k)
     for q in order:
         fwd[q].wait_recv()
         pfs[3, q] = pf(3, q)
@@ -684,6 +750,7 @@
         vm((rows, D), BF16), vm((rows, D), BF16), vm((D, 2 * L), BF16), vm((D, L), BF16), vm((7, 2, 2, DB // 4, 2 * L), BF16),
         near, near, near, wide, flat, flat, flat, flat, near, wide,
         near, near, vm((rows, 2 * L), BF16), vm((7, rows, 2 * L), BF16), vm((rows, DB), F32),
+        vm((rows, 2 * L), BF16), vm((6, 2, rows // NC, 2 * L), BF16), near, vm((rows, L), BF16), vm((6, 2, rows // NC, L), BF16),
         halo, halo, halo, halo, vm((K, L), F32), vm((1, L), F32),
         vm((L, rows), BF16), vm((2 * L, rows), BF16),
         vm((NO, Y, RB, L), BF16), vm((NN + 1, Y, RB, L), BF16),
@@ -697,7 +764,7 @@
         halo, vm((Y, PAD, L), F32), vm((PAD, L), BF16), vm((Z, PAD, L), BF16),
         pltpu.SemaphoreType.REGULAR((6,)),
         dma((4,)), dma((4,)), dma((4,)), *[dma((1,)) for _ in range(2)], *[dma((2,)) for _ in range(6)],
-        *[dma((1,)) for _ in range(4)], dma((1,)), dma((19,)), *[dma((1,)) for _ in range(24)],
+        *[dma((1,)) for _ in range(4)], dma((2,)), dma((19,)), dma((2,)), dma((1,)), dma((12,)), *[dma((1,)) for _ in range(5)], dma((NF,)), *[dma((1,)) for _ in range(18)],
     ]
     shapes = (
         jax.ShapeDtypeStruct((rows, DB), BF16),

time: 46.1 us -> 44.7 us (0.970)
  the two profiles are of different devices: /device:TPU:121 before, /device:TPU:2 now
where the time goes in v5:
time: 44.7 us; the launch traced here: 44.5 us
  Pallas kernels  43.9 us (98%)
  between operations  0.64 us (1%)
    pallas_call x1, Pallas kernels, shards(): pl.pallas_call(functools.partial(body, Z, Y, C, K), out_shape=shapes, in_...  43 us

profile of v5, /device:TPU:2, one launch (start us, length us, event | category | flops | bytes accessed | tf_op | source)
XLA Modules:
  0.0 44.5 jit_solution(10049396581412173725)
XLA Ops:
  0.6 43.0 %block_backward.1 = (bf16[1024,256]{1,0:T(8,128)(2,1)S(1)}, f32[64,128]{1,0:T(8,128)S(1)}, f32[64,128]{1,0:T(8,128)S(1)}, f32[64,128]{1,0:T(8,128)S(1)}, f32[31,128]{1,0:T(8,128)S(1)}, /*index=5*/f32[1,128]{1,0:T(1,128)S(1)}) custom-call(bf16[1024,2048]{1,0:T(8,128)(2,1)} %x_hbm.1, bf16[2048,128]{1,0:T(8,128)(2,1)} %vp_hbm.1, bf16[2048,128]{1,0:T(8,128)(2,1)} %gp_hbm.1, ...), custom_call_target="tpu_custom_call" | custom-call | tf_op jit(solution)/shard_map/block_backward/pallas_call | solution.py:782
  43.7 0.9 %write_out.1 = (bf16[1024,256]{1,0:T(8,128)(2,1)}, f32[64,128]{1,0:T(8,128)}, f32[64,128]{1,0:T(8,128)}, f32[64,128]{1,0:T(8,128)}, f32[31,128]{1,0:T(8,128)}, /*index=5*/f32[1,128]{1,0:T(1,128)}) custom-call(bf16[1024,256]{1,0:T(8,128)(2,1)S(1)} %get-tuple-element.18.refs_0_, f32[64,128]{1,0:T(8,128)S(1)} %get-tuple-element.19.refs_1_, ...), custom_call_target="tpu_custom_call" | custom-call | tf_op jit(solution)/shard_map/write_out/pallas_call | solution.py:793

commit v6 on v5

--- a/solution.py
+++ b/solution.py
@@ -742,7 +742,7 @@
     vm = pltpu.VMEM
     dma = pltpu.SemaphoreType.DMA
     hbm, vmem = pl.BlockSpec(memory_space=ANYWHERE), pl.BlockSpec(memory_space=pltpu.VMEM)
-    near, wide = vm((S * NP, L), F32), vm((S * HP, L), F32)
+    near, wide = vm((S * NP + T, L), F32), vm((S * HP + T + PAD, L), F32)
     flat = vm((T, S, L), F32)
     halo = vm((PAD, L), F32)
     stat, stats = vm((2, S, L), F32), vm((7, 2, S, L), F32)

time: 44.7 us -> 44.7 us (level)
  no operation moved by 1% of the time
where the time goes in v6:
time: 44.7 us; the launch traced here: 44.5 us
  Pallas kernels  43.9 us (98%)
  between operations  0.64 us (1%)
    pallas_call x1, Pallas kernels, shards(): pl.pallas_call(functools.partial(body, Z, Y, C, K), out_shape=shapes, in_...  43 us

profile of v6, /device:TPU:2, one launch (start us, length us, event | category | flops | bytes accessed | tf_op | source)
XLA Modules:
  0.0 44.5 jit_solution(13632027551676882748)
XLA Ops:
  0.6 43.0 %block_backward.1 = (bf16[1024,256]{1,0:T(8,128)(2,1)S(1)}, f32[64,128]{1,0:T(8,128)S(1)}, f32[64,128]{1,0:T(8,128)S(1)}, f32[64,128]{1,0:T(8,128)S(1)}, f32[31,128]{1,0:T(8,128)S(1)}, /*index=5*/f32[1,128]{1,0:T(1,128)S(1)}) custom-call(bf16[1024,2048]{1,0:T(8,128)(2,1)} %x_hbm.1, bf16[2048,128]{1,0:T(8,128)(2,1)} %vp_hbm.1, bf16[2048,128]{1,0:T(8,128)(2,1)} %gp_hbm.1, ...), custom_call_target="tpu_custom_call" | custom-call | tf_op jit(solution)/shard_map/block_backward/pallas_call | solution.py:782
  43.7 0.9 %write_out.1 = (bf16[1024,256]{1,0:T(8,128)(2,1)}, f32[64,128]{1,0:T(8,128)}, f32[64,128]{1,0:T(8,128)}, f32[64,128]{1,0:T(8,128)}, f32[31,128]{1,0:T(8,128)}, /*index=5*/f32[1,128]{1,0:T(1,128)}) custom-call(bf16[1024,256]{1,0:T(8,128)(2,1)S(1)} %get-tuple-element.18.refs_0_, f32[64,128]{1,0:T(8,128)S(1)} %get-tuple-element.19.refs_1_, ...), custom_call_target="tpu_custom_call" | custom-call | tf_op jit(solution)/shard_map/write_out/pallas_call | solution.py:793
